TPU v7x, 512 devices: a whole 4x4x16 slice. The times are simulated.
512 devices in a mesh: sp: 16 (over z), tp: 4 (over y), dp: 8 (over x, core).
Axes of the slice: x: 4, y: 4, z: 16, core: 2. Of those that a mesh axis runs over, the one named last changes fastest.
Arguments:
- latent: bfloat16 [32768, 2048], P(('dp', 'sp', 'tp')), parts along dimension 0, may hold values from -6 to 6
- context: bfloat16 [2048, 2048], P(('dp', 'sp')), parts along dimension 0, may hold values from -6 to 6
- cond: bfloat16 [16384], P(('dp', 'sp')), parts along dimension 0, may hold values from -6 to 6
- context_cond: bfloat16 [2048], P('sp'), may hold values from -6 to 6
- norm_gain: float32 [2048], replicated, may hold values from 0.1 to 1.9
- mod_shift: bfloat16 [2048, 2048], P('sp', 'tp'), may hold values from -0.125 to 0.125
- mod_scale: bfloat16 [2048, 2048], P('sp', 'tp'), may hold values from -0.125 to 0.125
- mod_gate: bfloat16 [2048, 2048], P('sp', 'tp'), may hold values from -0.125 to 0.125
- w_query: bfloat16 [2048, 1024], P(None, 'tp'), may hold values from -0.125 to 0.125
- w_key: bfloat16 [2048, 1024], P(None, 'tp'), may hold values from -0.125 to 0.125
- w_value: bfloat16 [2048, 1024], P(None, 'tp'), may hold values from -0.125 to 0.125
- query_gain: float32 [64], replicated, may hold values from 1.4 to 2.2
- key_gain: float32 [64], replicated, may hold values from 0.1 to 1.9
- mix_lambda: float32 [8], P('tp'), may hold values from 0.3 to 0.8
- context_lift: float32 [8], P('tp'), may hold values from 1.5 to 2.5
- value_gain: float32 [128], replicated, may hold values from 0.1 to 1.9
- w_out: bfloat16 [1024, 2048], P('tp'), may hold values from -0.1875 to 0.1875
Outputs:
- output: bfloat16 [32768, 2048], P(('dp', 'sp', 'tp')), parts along dimension 0
There are 8 independent parts, one for each index of `dp`. A program takes and returns all parts, laid end to end along the dimension named above; an argument that names none is the same for every part. Nothing has to cross between parts.
All inputs are finite; a program needn't handle non-finite values.
Results may differ from a plain program's by a relative error of at most 0.006.
Values may be sent and summed in bfloat16 or wider, within the bound.
A program may use at most 64 MiB of HBM per device.

v0:
```python
import jax
import jax.numpy as jnp
from jax import lax
from jax.sharding import PartitionSpec as P

GRID = 64


token_eps = 0.01
head_eps = 0.001
rope_base = 10000.0
head_factor = 0.8
key_block = 512


def copy_for_each(array, axis):
    copies = jnp.broadcast_to(array, (lax.axis_size(axis), *array.shape))
    return lax.all_to_all(copies, axis, split_axis=0, concat_axis=0, tiled=True)


def taken_together(array, axis):
    return copy_for_each(array, axis).sum(axis=0)


def in_order(tiles, dim):
    tiles = jnp.moveaxis(tiles, 0, dim)
    shape = tiles.shape
    return tiles.reshape(*shape[:dim], shape[dim] * shape[dim + 1], *shape[dim + 2 :])


def collect(array, axis, dim):
    tiles = copy_for_each(array, axis)
    return in_order(tiles, dim)


def sent_together(arrays, axis, dim, along):
    both = jnp.concatenate(arrays, axis=along)
    out, at, gathered = (lax.all_gather(both, axis, axis=dim, tiled=True), 0, [])
    for a in arrays:
        gathered.append(lax.slice_in_dim(out, at, at + a.shape[along], axis=along))
        at += a.shape[along]
    return tuple(gathered)


def cut_along(array, dim, devices):
    before, after = (array.shape[:dim], array.shape[dim + 1 :])
    return jnp.moveaxis(array.reshape(*before, devices, -1, *after), dim, 0)


def sum_at_owner(array, axis, dim):
    devices = lax.axis_size(axis)
    tiles = lax.all_to_all(cut_along(array, dim, devices), axis, 0, 0, tiled=True)
    return jnp.sum(tiles, axis=0)


def modulated_norm(row_block, gain_vector, shift_vector, scale_vector):
    values = row_block.astype(jnp.float32)
    inverse = lax.rsqrt(jnp.mean(values * values, axis=-1, keepdims=True) + token_eps)
    return (values * inverse * gain_vector * (1.0 + scale_vector) + shift_vector).astype(
        jnp.bfloat16
    )


def head_norm(values, gain_vector):
    inverse = lax.rsqrt(jnp.mean(values * values, axis=-1, keepdims=True) + token_eps)
    return values * inverse * gain_vector


def rotate(values, positions):
    quarter = values.shape[-1] // 4
    inverse = rope_base ** (-jnp.arange(quarter, dtype=jnp.float32) / quarter)
    grid_row = (positions // GRID).astype(jnp.float32)
    grid_col = (positions % GRID).astype(jnp.float32)
    angles = jnp.stack([grid_row[:, None] * inverse, grid_col[:, None] * inverse], axis=1)
    cosine_table = jnp.cos(angles)[:, None, None]
    sine_table = jnp.sin(angles)[:, None, None]
    halves = values.reshape(values.shape[:3] + (2, 2, quarter))
    front_half = halves[..., 0, :]
    back_half = halves[..., 1, :]
    turned = jnp.stack(
        [
            front_half * cosine_table - back_half * sine_table,
            back_half * cosine_table + front_half * sine_table,
        ],
        axis=-2,
    )
    return turned.reshape(values.shape)


def project_heads(row_block, weight, gain_vector, positions, factor):
    row_count = row_block.shape[0]
    head_width = gain_vector.shape[0]
    product = jnp.dot(row_block, weight, preferred_element_type=jnp.float32)
    shaped = head_norm(product.reshape(row_count, -1, 2, head_width), gain_vector)
    if positions is not None:
        shaped = rotate(shaped, positions)
    return (shaped * factor).astype(jnp.bfloat16).reshape(row_count, -1)


def accumulate(running, queries, key_slab, value_slab, lift_rows):
    numerator, totals = running
    head_count = lift_rows.shape[0]
    head_width = queries.shape[1] // (2 * head_count)
    shaped_query = queries.reshape(queries.shape[0], head_count, 2, head_width)
    shaped_keys = key_slab.reshape(key_slab.shape[0], head_count, 2, head_width)
    shaped_values = value_slab.reshape(value_slab.shape[0], head_count, -1)
    scores = jnp.einsum(
        "qhmd,phmd->mhqp", shaped_query, shaped_keys, preferred_element_type=jnp.float32
    )
    weights = jnp.exp(scores + lift_rows[None, :, None, :])
    totals = totals + jnp.sum(weights, axis=-1)
    numerator = numerator + jnp.einsum(
        "mhqp,phe->mhqe",
        weights.astype(jnp.bfloat16),
        shaped_values,
        preferred_element_type=jnp.float32,
    )
    return (numerator, totals)


def accumulate_blocks(running, queries, key_slab, value_slab, lift_rows):
    row_count = key_slab.shape[0]
    full_blocks = row_count // key_block
    covered = full_blocks * key_block
    head_count = lift_rows.shape[0]
    slabs = (
        key_slab[:covered].reshape(full_blocks, key_block, -1),
        value_slab[:covered].reshape(full_blocks, key_block, -1),
        jnp.transpose(
            lift_rows[:, :covered].reshape(head_count, full_blocks, key_block), (1, 0, 2)
        ),
    )

    def scan_step(inside, slab):
        return (accumulate(inside, queries, slab[0], slab[1], slab[2]), None)

    running = lax.scan(scan_step, running, slabs)[0]
    running = accumulate(
        running, queries, key_slab[covered:], value_slab[covered:], lift_rows[:, covered:]
    )
    return running


def on_device(
    latent,
    context,
    cond,
    context_cond,
    norm_gain,
    mod_shift,
    mod_scale,
    mod_gate,
    w_query,
    w_key,
    w_value,
    query_gain,
    key_gain,
    mix_lambda,
    context_lift,
    value_gain,
    w_out,
):
    cond_act = jax.nn.silu(cond.astype(jnp.float32)).astype(jnp.bfloat16)
    context_act = jax.nn.silu(context_cond.astype(jnp.float32)).astype(jnp.bfloat16)
    both_acts = jnp.stack([cond_act, context_act])
    shifts = jnp.dot(both_acts, mod_shift, preferred_element_type=jnp.float32)
    scales = jnp.dot(both_acts, mod_scale, preferred_element_type=jnp.float32)
    gates = jnp.dot(cond_act[None, :], mod_gate, preferred_element_type=jnp.float32)
    partial_mod = jnp.concatenate([shifts, scales, gates], axis=0)
    summed = taken_together(partial_mod, "sp")
    modulation = collect(summed, "tp", 1)
    normed = modulated_norm(latent, norm_gain, modulation[0], modulation[2])
    context_normed = modulated_norm(context, norm_gain, modulation[1], modulation[3])
    local_rows = latent.shape[0]
    offset = lax.axis_index("sp") * (local_rows * lax.axis_size("tp"))
    head_width = query_gain.shape[0]
    pieces = lax.all_gather(normed, "tp", axis=0, tiled=True)
    positions = offset + jnp.arange(pieces.shape[0], dtype=jnp.int32)
    query_part = project_heads(pieces, w_query, query_gain, positions, head_width ** (-0.5))
    key_part = project_heads(pieces, w_key, key_gain, positions, 1.0)
    value_part = jnp.dot(pieces, w_value, preferred_element_type=jnp.float32).astype(jnp.bfloat16)
    projected = jnp.concatenate([query_part, key_part, value_part], axis=1)
    qk_width = w_query.shape[1]
    queries = projected[:, :qk_width]
    latent_keys = projected[:, qk_width : 2 * qk_width]
    latent_values = projected[:, 2 * qk_width :]
    heads_here = mix_lambda.shape[0]
    query_rows = queries.shape[0]
    value_width = latent_values.shape[1] // heads_here
    empty = (
        jnp.zeros((2, heads_here, query_rows, value_width), jnp.float32),
        jnp.zeros((2, heads_here, query_rows), jnp.float32),
    )
    latent_count = latent_keys.shape[0]
    own_keys = project_heads(context_normed, w_key, key_gain, None, 1.0)
    own_values = jnp.dot(context_normed, w_value, preferred_element_type=jnp.float32).astype(
        jnp.bfloat16
    )
    shard_keys = jnp.concatenate([latent_keys, own_keys], axis=0)
    shard_values = jnp.concatenate([latent_values, own_values], axis=0)
    extra_rows = own_keys.shape[0]
    shard_rows = latent_count + extra_rows
    pieces = sent_together((shard_keys, shard_values), "sp", 0, 1)
    row_index = jnp.arange(pieces[0].shape[0], dtype=jnp.int32) % shard_rows
    lift_rows = jnp.where(row_index[None, :] >= latent_count, context_lift[:, None], 0.0)
    numerator, totals = accumulate_blocks(empty, queries, pieces[0], pieces[1], lift_rows)
    ratios = numerator / totals[..., None]
    mixed_heads = ratios[0] - mix_lambda[:, None, None] * ratios[1]
    inverse = lax.rsqrt(jnp.mean(mixed_heads * mixed_heads, axis=-1, keepdims=True) + head_eps)
    head_out = (mixed_heads * inverse * value_gain * head_factor).astype(jnp.bfloat16)
    out_weight = w_out.reshape(heads_here, value_width, w_out.shape[1])
    mixture = sum_at_owner(
        jnp.einsum("hqe,hed->qd", head_out, out_weight, preferred_element_type=jnp.float32), "tp", 0
    )
    return (latent.astype(jnp.float32) + modulation[4] * mixture).astype(jnp.bfloat16)


def solution(mesh):
    placed = (
        P(("dp", "sp", "tp"), None),
        P(("dp", "sp"), None),
        P(("dp", "sp")),
        P("sp"),
        P(),
        P("sp", "tp"),
        P("sp", "tp"),
        P("sp", "tp"),
        P(None, "tp"),
        P(None, "tp"),
        P(None, "tp"),
        P(),
        P(),
        P("tp"),
        P("tp"),
        P(),
        P("tp", None),
    )
    return jax.shard_map(
        on_device,
        mesh=mesh,
        in_specs=placed,
        out_specs=P(("dp", "sp", "tp"), None),
        check_vma=False,
    )
```

profile of v0, /device:TPU:6, one launch (start us, length us, event | category | flops | bytes accessed | tf_op | source)
XLA Modules:
  0.0 231.4 jit_solution(1074336177027201900)
XLA Ops:
  6.5 0.8 convert_bitcast_fusion
  7.4 1.1 fusion.33
  8.4 1.0 fusion.36
  9.5 1.0 fusion.37
  10.5 0.7 broadcast_in_dim.21
  11.3 15.2 %all-to-all-start = ((f32[16,5,512]{2,1,0:T(8,128)}), f32[16,5,512]{2,1,0:T(8,128)}, u32[]{:S(2)}, u32[]{:S(2)}) async-start(f32[16,5,512]{2,1,0:T(8,128)} %broadcast_in_dim.21), calls=%async_computation | async-start | bytes 524288 | tf_op jit(solution)/shard_map/all_to_all | solution.py:18
  26.5 0.6 fusion.30
  27.1 1.1 fusion.7
  28.2 0.5 add_rsqrt_fusion.5
  28.7 16.2 %all-to-all-done = f32[16,5,512]{2,1,0:T(8,128)} async-done(((f32[16,5,512]{2,1,0:T(8,128)}), f32[16,5,512]{2,1,0:T(8,128)}, u32[]{:S(2)}, u32[]{:S(2)}) %all-to-all-start) | async-done | bytes 163872 | tf_op jit(solution)/shard_map/all_to_all | solution.py:18
  45.0 1.0 reduce_sum.90
  45.9 0.6 broadcast_in_dim.22
  46.6 4.5 %all-to-all-start.1 = ((f32[4,5,512]{2,1,0:T(8,128)}), f32[4,5,512]{2,1,0:T(8,128)S(1)}, u32[]{:S(2)}, u32[]{:S(2)}) async-start(f32[4,5,512]{2,1,0:T(8,128)} %broadcast_in_dim.22), calls=%async_computation.1 | async-start | bytes 131072 | tf_op jit(solution)/shard_map/all_to_all | solution.py:18
  51.0 0.6 multiply_power_fusion
  51.6 1.3 mul.366
  52.9 1.3 mul.331
  54.2 0.7 mul.358
  54.9 0.7 mul.359
  55.6 1.1 all-to-all-done.1
  56.7 0.6 fusion.44
  57.3 1.5 fusion.11
  58.8 0.7 broadcast_multiply_fusion.1
  59.6 0.8 fusion.25
  60.5 1.6 fusion.45
  62.7 1.3 multiply_convert_fusion.1
  64.1 1.5 convolution_convert_fusion.1
  65.6 19.4 %all-gather.3.cloned.1.call-done = bf16[256,2048]{1,0:T(8,128)(2,1)} async-done(((bf16[64,2048]{1,0:T(8,128)(2,1)}), bf16[256,2048]{1,0:T(8,128)(2,1)}) %all-gather.3.cloned.1.call-update) | async-done | bytes 1048592 | tf_op jit(solution)/shard_map/all_gather | solution.py:177
  85.0 2.2 bitcast_reduce_fusion.1
  87.2 0.5 bitcast_reduce_fusion.2
  88.0 0.7 multiply_subtract_fusion
  88.7 0.7 pad_maximum_fusion
  89.4 1.7 copy.89
  91.1 0.4 convolution_convert_fusion
  91.5 0.4 copy-done.7
  92.0 0.7 maximum_maximum_fusion
  92.8 0.7 broadcast_select_fusion
  93.5 0.9 fusion.16
  94.5 77.1 %all-gather.5.cloned.1.call-done = bf16[4352,512]{1,0:T(8,128)(2,1)} async-done(((bf16[272,512]{1,0:T(8,128)(2,1)}), bf16[4352,512]{1,0:T(8,128)(2,1)}) %all-gather.5.cloned.1.call-update) | async-done | bytes 4456464 | tf_op jit(solution)/shard_map/all_gather | solution.py:38
  171.6 1.0 fusion.41
  172.8 4.5 %fusion.42 = (bf16[4096,256]{1,0:T(8,128)(2,1)}, bf16[4096,256]{1,0:T(8,128)(2,1)}) fusion(bf16[4352,512]{1,0:T(8,128)(2,1)} %all-gather.5.cloned.1.call-done), kind=kLoop, calls=%fused_computation.102 | loop fusion | bytes 8388608 | tf_op jit(solution)/shard_map/slice | solution.py:127
  177.3 21.7 %while.13 = (s32[]{:T(128)}, f32[2,2,256,128]{2,3,0,1:T(8,128)S(1)}, f32[2,2,256]{2,1,0:T(2,128)S(1)}, bf16[8,512,256]{2,1,0:T(8,128)(2,1)}, bf16[8,512,256]{2,1...) while((s32[]{:T(128)}, ...), condition=%wide.region_8.9_spmd.clone, body=%wide.region_6.8_spmd.clone.sunk | while | flops 203686912 | bytes 10125432 | solution.py:137
  177.3 1.1 constant_dynamic-slice_fusion.3
  178.7 0.6 bitcast_convert_fusion.2
  179.6 0.4 bitcast_reduce_fusion.4
  180.0 1.1 constant_dynamic-slice_fusion.3
  181.4 0.6 bitcast_convert_fusion.2
  182.7 1.1 constant_dynamic-slice_fusion.3
  184.1 0.6 bitcast_convert_fusion.2
  185.0 0.4 bitcast_reduce_fusion.4
  185.4 1.1 constant_dynamic-slice_fusion.3
  186.8 0.6 bitcast_convert_fusion.2
  188.1 1.1 constant_dynamic-slice_fusion.3
  189.5 0.6 bitcast_convert_fusion.2
  190.9 1.1 constant_dynamic-slice_fusion.3
  192.2 0.6 bitcast_convert_fusion.2
  193.6 1.1 constant_dynamic-slice_fusion.3
  194.9 0.6 bitcast_convert_fusion.2
  196.3 1.1 constant_dynamic-slice_fusion.3
  197.6 0.6 bitcast_convert_fusion.2
  199.0 0.4 fusion.43
  200.1 0.4 convolution_bitcast_fusion.1
  200.5 21.2 %all_to_all.15 = f32[4,64,2048]{2,1,0:T(8,128)S(1)} all-to-all(f32[4,64,2048]{2,1,0:T(8,128)S(1)} %convolution_bitcast_fusion.1), channel_id=1, replica_groups=mesh['sp'=16,'tp'=4,'dp'=8] {'tp'}, dimensions={0} | all-to-all | bytes 4194304 | tf_op jit(solution)/shard_map/all_to_all | solution.py:52
  221.8 1.0 reduce_sum.98
  222.7 1.8 fusion.12
  (121 shorter events, 9.3 us)
Async XLA Ops:
  6.5 193.5 %copy-start = (bf16[256,2048]{1,0:T(8,128)(2,1)S(1)}, bf16[256,2048]{1,0:T(8,128)(2,1)}, u32[]{:S(2)}) copy-start(bf16[256,2048]{1,0:T(8,128)(2,1)} %param.35) | copy-start | bytes 3145732
  6.5 50.8 %copy-start.5 = (bf16[64,2048]{1,0:T(8,128)(2,1)S(1)}, bf16[64,2048]{1,0:T(8,128)(2,1)}, u32[]{:S(2)}) copy-start(bf16[64,2048]{1,0:T(8,128)(2,1)} %param.19) | copy-start | bytes 786436
  6.5 50.8 %copy-start.11 = (f32[2048]{0:T(1024)S(1)}, f32[2048]{0:T(1024)}, u32[]{:S(2)}) copy-start(f32[2048]{0:T(1024)} %param.23) | copy-start | bytes 24580
  6.5 53.8 %copy-start.6 = (bf16[16,2048]{1,0:T(8,128)(2,1)S(1)}, bf16[16,2048]{1,0:T(8,128)(2,1)}, u32[]{:S(2)}) copy-start(bf16[16,2048]{1,0:T(8,128)(2,1)} %param.20) | copy-start | bytes 196612
  6.5 54.0 %copy-start.2 = (bf16[2048,256]{1,0:T(8,128)(2,1)S(1)}, bf16[2048,256]{1,0:T(8,128)(2,1)}, u32[]{:S(2)}) copy-start(bf16[2048,256]{1,0:T(8,128)(2,1)} %param.28) | copy-start | bytes 3145732
  10.5 53.5 %copy-start.3 = (bf16[2048,256]{1,0:T(8,128)(2,1)S(1)}, bf16[2048,256]{1,0:T(8,128)(2,1)}, u32[]{:S(2)}) copy-start(bf16[2048,256]{1,0:T(8,128)(2,1)} %param.29) | copy-start | bytes 3145732
  11.3 33.7 %all-to-all-start = ((f32[16,5,512]{2,1,0:T(8,128)}), f32[16,5,512]{2,1,0:T(8,128)}, u32[]{:S(2)}, u32[]{:S(2)}) async-start(f32[16,5,512]{2,1,0:T(8,128)} %broadcast_in_dim.21), calls=%async_computation | async-start | bytes 524288 | tf_op jit(solution)/shard_map/all_to_all | solution.py:18
  46.6 10.1 %all-to-all-start.1 = ((f32[4,5,512]{2,1,0:T(8,128)}), f32[4,5,512]{2,1,0:T(8,128)S(1)}, u32[]{:S(2)}, u32[]{:S(2)}) async-start(f32[4,5,512]{2,1,0:T(8,128)} %broadcast_in_dim.22), calls=%async_computation.1 | async-start | bytes 131072 | tf_op jit(solution)/shard_map/all_to_all | solution.py:18
  51.0 33.9 %all-gather.3.cloned.1.call-start = ((), (), s32[]{:S(2)}) async-start(), calls=%async_computation.3 | async-start | bytes 1310720 | tf_op jit(solution)/shard_map/all_gather | solution.py:177
  57.3 6.8 %copy-start.12 = (f32[1,4,512]{2,0,1:T(1,128)S(1)}, f32[1,4,512]{2,0,1:T(1,128)}, u32[]{:S(2)}) copy-start(f32[1,4,512]{2,0,1:T(1,128)} %get-tuple-element.141) | copy-start | bytes 24580
  58.8 112.8 %all-gather.5.cloned.1.call-start = ((), (), s32[]{:S(2)}) async-start(), calls=%async_computation.4 | async-start | bytes 4734976 | tf_op jit(solution)/shard_map/all_gather | solution.py:38
  60.5 1.7 copy-start.19
  65.6 22.2 %copy-start.17 = (f32[2,2,16]{2,1,0:T(2,128)S(1)}, f32[2,2,16]{2,1,0:T(2,128)}, u32[]{:S(2)}) copy-start(f32[2,2,16]{2,1,0:T(2,128)} %mul.366) | copy-start | bytes 772
  65.6 22.3 %copy-start.16 = (f32[2,2,16]{2,1,0:T(2,128)S(1)}, f32[2,2,16]{2,1,0:T(2,128)}, u32[]{:S(2)}) copy-start(f32[2,2,16]{2,1,0:T(2,128)} %mul.331) | copy-start | bytes 772
  85.0 2.2 copy-start.1
  87.1 0.8 copy-start.9
  87.1 0.8 copy-start.10
  87.7 3.3 %copy-start.4 = (bf16[2048,256]{1,0:T(8,128)(2,1)S(1)}, bf16[2048,256]{1,0:T(8,128)(2,1)}, u32[]{:S(2)}) copy-start(bf16[2048,256]{1,0:T(8,128)(2,1)} %param.29) | copy-start | bytes 3145732
  87.9 3.7 %copy-start.13 = (bf16[16,256]{1,0:T(8,128)(2,1)S(1)}, bf16[16,256]{1,0:T(8,128)(2,1)}, u32[]{:S(2)}) copy-start(bf16[16,256]{1,0:T(8,128)(2,1)} %convolution_convert_fusion.1) | copy-start | bytes 24580
  87.9 3.7 %copy-start.15 = (bf16[16,256]{1,0:T(8,128)(2,1)S(1)}, bf16[16,256]{1,0:T(8,128)(2,1)}, u32[]{:S(2)}) copy-start(bf16[16,256]{1,0:T(8,128)(2,1)} %multiply_convert_fusion.1) | copy-start | bytes 24580
  91.1 0.9 copy-start.7
  93.5 83.8 %copy-start.8 = (f32[2,4352]{1,0:T(2,128)}, f32[2,4352]{1,0:T(2,128)S(1)}, u32[]{:S(2)}) copy-start(f32[2,4352]{1,0:T(2,128)S(1)} %broadcast_select_fusion) | copy-start | bytes 104452
  177.3 21.7 %slice-start = ((f32[2,4352]{1,0:T(2,128)}), f32[2,256]{1,0:T(2,128)S(1)}, s32[]{:S(2)}) async-start(f32[2,4352]{1,0:T(2,128)} %copy-done.8), calls=%async_computation.5 | async-start | bytes 4096 | tf_op jit(solution)/shard_map/slice | solution.py:139
  199.0 0.7 copy-start.18
  199.0 0.8 copy-start.20
  221.8 1.0 copy-start.14
Sparse Core Ops, SparseCore 0:
  58.9 26.0 all-gather.2
  92.9 78.6 all-gather.4
where the time goes:
time: 232 us; the launch traced here: 231 us
  waiting for transfers between devices  114 us (49%)
  local copies, waits for them, and re-layouts  24.7 us (11%)
  blocking collectives  21.2 us (9%)
  other arithmetic  19.8 us (9%)
  starting transfers between devices  19.8 us (9%)
  matrix products  17.8 us (8%)
  between operations  13.8 us (6%)
    all_gather x1, waiting for transfers between devices, sent_together(): lax.all_gather(both, axis, axis=dim, tiled=True)  77.1 us
    all_to_all x1, blocking collectives, sum_at_owner(): lax.all_to_all(cut_along(array, dim, devices), axis, 0, 0, tiled=True)  21.2 us
    all_to_all x2, starting transfers between devices, copy_for_each(): return lax.all_to_all(copies, axis, split_axis=0, concat_axis=0, tiled=True)  19.7 us
    all_gather x1, waiting for transfers between devices, on_device(): pieces = lax.all_gather(normed, 'tp', axis=0, tiled=True)  19.4 us
    all_to_all x2, waiting for transfers between devices, copy_for_each(): return lax.all_to_all(copies, axis, split_axis=0, concat_axis=0, tiled=True)  17.3 us
    dynamic_slice x24, local copies, waits for them, and re-layouts, accumulate_blocks(): running = lax.scan(scan_step, running, slabs)[0]  10.8 us
    dot_general x9, matrix products, accumulate(): jnp.einsum('qhmd,phmd->mhqp', shaped_query, shaped_keys, preferred_elemen...  4.96 us
  transfers between devices with their start and end apart: 4, of which 4 were waited for; matrix products, arithmetic and copies ran while one was open for 7% of the time, Pallas kernels for 0%

commit v1 on v0

v1 whole, which is shorter than its diff:
```python
import functools

import jax
import jax.numpy as jnp
import numpy as np
from jax import lax
from jax.experimental import pallas as pl
from jax.experimental.pallas import tpu as pltpu
from jax.sharding import PartitionSpec as P

GRID = 64
token_eps = 0.01
head_eps = 0.001
rope_base = 10000.0
head_factor = 0.8
MESH = pl.DeviceIdType.MESH
F32 = jnp.float32
BF16 = jnp.bfloat16


def rope_table(head_width):
    quarter = head_width // 4
    inverse = np.float32(rope_base) ** (-np.arange(quarter, dtype=np.float32) / np.float32(quarter))
    angles = (np.arange(GRID, dtype=np.float32)[:, None] * inverse).astype(np.float64)
    cos, sin = np.cos(angles), np.sin(angles)
    zero = np.zeros_like(cos)
    cos_row = np.concatenate([cos, cos, zero, zero], 1)
    cos_col = np.concatenate([zero, zero, cos, cos], 1)
    sin_row = np.concatenate([-sin, sin, zero, zero], 1)
    sin_col = np.concatenate([zero, zero, -sin, sin], 1)
    table = np.stack([np.stack([cos_row, cos_col]), np.stack([sin_row, sin_col])])
    return np.tile(table, (1, 1, 1, 2)).astype(np.float32)


def silu(v):
    return v / (1.0 + jnp.exp(-v))


def kernel(
    dims,
    latent, context, cond, cctx, gain, msh, msc, mga, qg, kg, vg, lam, lift, rope, wq_h, wk_h, wv_h, wo_h,
    out,
    wq, wk, wv, wo, lat, normed, inv, part, sums, far, full, cosb, sinb, qz, kbuf, vbuf, numer, tot, hosend, ho,
    lsem, p_send, p_recv, f_send, f_recv, c_send, c_recv, y_send, y_recv, w_send, w_recv, r_send, r_recv, o_send, o_recv,
):
    Z, Y = dims
    z, y = lax.axis_index("sp"), lax.axis_index("tp")

    def zz(d):
        return lax.rem(z + (d + Z), Z)

    def yy(d):
        return lax.rem(y + (d + Y), Y)

    loads = [
        pltpu.make_async_copy(wk_h, wk, lsem.at[0]),
        pltpu.make_async_copy(wv_h, wv, lsem.at[1]),
        pltpu.make_async_copy(wq_h, wq, lsem.at[2]),
        pltpu.make_async_copy(wo_h, wo.at[y], lsem.at[3]),
    ]
    for copy in loads:
        copy.start()

    barrier = pltpu.get_barrier_semaphore()
    z_peers = [1, 2, 3, 4, 5, -1, -2, -3, -4, -5]
    for d in z_peers:
        pl.semaphore_signal(barrier, inc=1, device_id={"sp": zz(d)}, device_id_type=MESH)
    for d in (1, 2, 3):
        pl.semaphore_signal(barrier, inc=1, device_id={"tp": yy(d)}, device_id_type=MESH)

    rows16 = lax.broadcasted_iota(jnp.int32, (16, 128), 0)
    a0 = silu(cond[...].astype(F32))
    a1 = silu(cctx[...].astype(F32))
    acts = jnp.where(rows16 == 0, a0, jnp.where(rows16 == 1, a1, 0.0)).astype(BF16)
    p_sh = jnp.dot(acts, msh[...], preferred_element_type=F32)
    p_sc = jnp.dot(acts, msc[...], preferred_element_type=F32)
    p_ga = jnp.dot(acts, mga[...], preferred_element_type=F32)
    part[0, 0:1, :] = p_sh[0:1]
    part[0, 1:2, :] = p_sc[0:1]
    part[0, 2:3, :] = p_ga[0:1]
    part[0, 3:4, :] = p_sh[1:2]
    part[0, 4:5, :] = p_sc[1:2]
    part[0, 5:8, :] = jnp.zeros((3, part.shape[2]), F32)

    pl.semaphore_wait(barrier, len(z_peers) + 3)

    def copy_to(src, dst, ssem, rsem, **where):
        return pltpu.make_async_remote_copy(
            src_ref=src, dst_ref=dst, send_sem=ssem, recv_sem=rsem, device_id=where, device_id_type=MESH
        )

    offs = [-3, 3, -2, 2, -1, 1]
    stage1 = []
    for n, d in enumerate(offs):
        c = copy_to(part.at[0], part.at[n + 1], p_send.at[n], p_recv.at[n], sp=zz(-d))
        c.start()
        stage1.append(c)

    rows = latent.shape[0]
    half = rows // 2
    top, bottom = pl.ds(0, half), pl.ds(half, half)

    def y_copies(src, slots, send, recv, first, second):
        return [
            copy_to(src.at[first], slots.at[y, first], send.at[0], recv.at[0], tp=yy(1)),
            copy_to(src.at[second], slots.at[y, second], send.at[1], recv.at[1], tp=yy(-1)),
            copy_to(src.at[second], slots.at[y, second], send.at[2], recv.at[2], tp=yy(1)),
            copy_to(src.at[first], slots.at[y, first], send.at[3], recv.at[3], tp=yy(-1)),
        ]

    def y_forward(slots, send, recv, first, second):
        return [
            copy_to(slots.at[yy(-1), first], slots.at[yy(-1), first], send.at[4], recv.at[4], tp=yy(1)),
            copy_to(slots.at[yy(1), second], slots.at[yy(1), second], send.at[5], recv.at[5], tp=yy(-1)),
        ]

    lat_sends = y_copies(latent, lat, y_send, y_recv, top, bottom)
    for c in lat_sends:
        c.start()
    lat[y] = latent[...]

    width = wq.shape[1]
    hw = qg.shape[1]
    gi = lax.broadcasted_iota(jnp.int32, (width, width), 0) // hw
    gj = lax.broadcasted_iota(jnp.int32, (width, width), 1) // hw
    average = jnp.where(gi == gj, 1.0 / hw, 0.0).astype(BF16)
    LR = Y * rows
    CR = context.shape[0]
    for k in range(Y):
        at = pl.ds(k * rows, rows)
        cosb[at, :] = rope[0, 0, pl.ds(Y * z + k, 1), :] + rope[0, 1]
        sinb[at, :] = rope[1, 0, pl.ds(Y * z + k, 1), :] + rope[1, 1]
    cosb[pl.ds(LR, CR), :] = jnp.ones((CR, 128), F32)
    sinb[pl.ds(LR, CR), :] = jnp.zeros((CR, 128), F32)

    def mean_square(x):
        xf = x.astype(F32)
        ms = jnp.mean(xf * xf, axis=-1, keepdims=True)
        return jnp.broadcast_to(lax.rsqrt(ms + token_eps), (x.shape[0], 128))

    inv[pl.ds(LR, CR), :] = mean_square(context[...])

    for c in stage1:
        c.wait_recv()
    sums[0] = part[0] + part[5] + part[3] + part[1]
    sums[1] = part[0] + part[6] + part[4] + part[2]
    stage2 = [
        copy_to(sums.at[1], far.at[2], f_send.at[2], f_recv.at[2], sp=zz(-5)),
        copy_to(sums.at[0], far.at[0], f_send.at[0], f_recv.at[0], sp=zz(4)),
        copy_to(sums.at[1], far.at[1], f_send.at[1], f_recv.at[1], sp=zz(-1)),
    ]
    for c in stage2:
        c.start()

    lat_sends[0].wait_recv()
    lat_sends[1].wait_recv()
    lat_forward = y_forward(lat, y_send, y_recv, top, bottom)
    for c in lat_forward:
        c.start()
    inv[pl.ds(y * rows, rows), :] = mean_square(latent[...])
    lat_sends[2].wait_recv()
    lat_sends[3].wait_recv()
    for d in (1, -1):
        inv[pl.ds(yy(d) * rows, rows), :] = mean_square(lat[yy(d)])

    for c in stage2:
        c.wait_recv()
    full[y] = sums[0] + far[0] + far[1] + far[2]
    stage3 = []
    for n, d in enumerate((2, 1, 3)):
        c = copy_to(full.at[y], full.at[y], c_send.at[n], c_recv.at[n], tp=yy(d))
        c.start()
        stage3.append(c)
    for c in lat_forward:
        c.wait_recv()
    inv[pl.ds(yy(2) * rows, rows), :] = mean_square(lat[yy(2)])
    for c in stage3:
        c.wait_recv()

    cb = full.shape[2]
    for b in range(Y):
        cols = pl.ds(b * cb, cb)
        a = gain[:, cols] * (1.0 + full[b, 1:2, :])
        s = full[b, 0:1, :]
        for k in range(Y):
            v = inv[pl.ds(k * rows, rows), :]
            v = jnp.concatenate([v] * (cb // 128), axis=1)
            normed[pl.ds(k * rows, rows), cols] = (lat[k, :, cols].astype(F32) * v * a + s).astype(BF16)
        a = gain[:, cols] * (1.0 + full[b, 4:5, :])
        s = full[b, 3:4, :]
        v = inv[pl.ds(LR, CR), :]
        v = jnp.concatenate([v] * (cb // 128), axis=1)
        normed[pl.ds(LR, CR), cols] = (context[:, cols].astype(F32) * v * a + s).astype(BF16)

    lane = lax.broadcasted_iota(jnp.int32, (1, 128), 1)
    q4 = hw // 4
    is_x = (lane // q4) % 2 == 0

    def head_norm(u, g):
        sq = u * u
        hi = sq.astype(BF16)
        lo = (sq - hi.astype(F32)).astype(BF16)
        ms = jnp.dot(hi, average, preferred_element_type=F32) + jnp.dot(lo, average, preferred_element_type=F32)
        return u * lax.rsqrt(ms + token_eps) * g

    def turn(t, n):
        other = jnp.where(is_x, pltpu.roll(t, 128 - q4, 1), pltpu.roll(t, q4, 1))
        return t * cosb[pl.ds(0, n), :] + other * sinb[pl.ds(0, n), :]

    heads = width // 128
    g2 = jnp.concatenate([kg[...]] * (width // hw), axis=1)
    loads[0].wait()
    u = head_norm(jnp.dot(normed[...], wk[...], preferred_element_type=F32), g2)
    for h in range(heads):
        kbuf[z, :, h * 128 : (h + 1) * 128] = turn(u[:, h * 128 : (h + 1) * 128], LR + CR).astype(BF16)

    def ring(step, direction, which):
        buf = kbuf if which == 0 else vbuf
        slot = lax.rem(z - direction * step + Z, Z)
        to = lax.rem(z + direction + Z, Z)
        side = 0 if direction == 1 else 1
        return copy_to(
            buf.at[slot], buf.at[slot], r_send.at[side, which, step], r_recv.at[side, which, step], sp=to
        )

    for direction in (1, -1):
        ring(0, direction, 0).start()
    loads[1].wait()
    vbuf[z] = jnp.dot(normed[...], wv[...], preferred_element_type=F32).astype(BF16)
    for direction in (1, -1):
        ring(0, direction, 1).start()

    loads[2].wait()
    g2 = jnp.concatenate([qg[...]] * (width // hw), axis=1)
    u = head_norm(jnp.dot(normed[pl.ds(0, LR), :], wq[...], preferred_element_type=F32), g2)
    for h in range(heads):
        t = turn(u[:, h * 128 : (h + 1) * 128], LR) * (hw ** -0.5)
        qz[h, pl.ds(0, LR), :] = jnp.where(lane < hw, t, 0.0).astype(BF16)
        qz[h, pl.ds(LR, LR), :] = jnp.where(lane < hw, 0.0, t).astype(BF16)

    wh = wo.shape[1] // 2
    loads[3].wait()
    wo_sends = y_copies(wo.at[y], wo, w_send, w_recv, pl.ds(0, wh), pl.ds(wh, wh))
    for c in wo_sends:
        c.start()

    numer[...] = jnp.zeros_like(numer)
    tot[...] = jnp.zeros_like(tot)

    def attend(h, keys, values, extra):
        s = lax.dot_general(qz[h], keys, (((1,), (1,)), ((), ())), preferred_element_type=F32)
        if extra is not None:
            s = s + extra
        w = jnp.exp(s)
        t = w[:, 0:128]
        for j in range(1, w.shape[1] // 128):
            t = t + w[:, j * 128 : (j + 1) * 128]
        tot[h] = tot[h] + t
        numer[h] = numer[h] + jnp.dot(w.astype(BF16), values, preferred_element_type=F32)

    def attend_slot(slot):
        def one(h, carry):
            hc = pl.ds(pl.multiple_of(h * 128, 128), 128)
            attend(h, kbuf[slot, pl.ds(0, LR), hc], vbuf[slot, pl.ds(0, LR), hc], None)
            return carry

        lax.fori_loop(0, heads, one, 0)

    attend_slot(z)
    last = Z // 2

    def hop(s, carry):
        for which in (0, 1):
            for direction in (1, -1):
                ring(s - 1, direction, which).wait_recv()
                ring(s, direction, which).start()
        attend_slot(lax.rem(z - s + Z, Z))
        attend_slot(lax.rem(z + s, Z))
        return carry

    mid = last // 2
    lax.fori_loop(1, mid, hop, 0)
    wo_sends[0].wait_recv()
    wo_sends[1].wait_recv()
    wo_forward = y_forward(wo, w_send, w_recv, pl.ds(0, wh), pl.ds(wh, wh))
    for c in wo_forward:
        c.start()
    lax.fori_loop(mid, last - 1, hop, 0)
    s = last - 1
    for direction in (1, -1):
        ring(s - 1, direction, 0).wait_recv()
        if direction == 1:
            ring(s, direction, 0).start()
    for direction in (1, -1):
        ring(s - 1, direction, 1).wait_recv()
        if direction == -1:
            ring(s, direction, 1).start()
    attend_slot(lax.rem(z - s + Z, Z))
    attend_slot(lax.rem(z + s, Z))
    ring(s, 1, 0).wait_recv()
    ring(s, -1, 1).wait_recv()
    attend_slot(lax.rem(z + last, Z))

    for h in range(heads):
        hc = slice(h * 128, (h + 1) * 128)
        keys = kbuf[:, pl.ds(LR, CR), hc].reshape(Z * CR, 128)
        values = vbuf[:, pl.ds(LR, CR), hc].reshape(Z * CR, 128)
        attend(h, keys, values, lift[h])

    for h in range(heads):
        total = jnp.sum(tot[h], axis=-1, keepdims=True)
        ratio = numer[h] / total
        mixed = ratio[0:LR] - lam[h] * ratio[LR : 2 * LR]
        ms = jnp.mean(mixed * mixed, axis=-1, keepdims=True)
        res = (mixed * lax.rsqrt(ms + head_eps) * vg[...] * head_factor).astype(BF16)
        for k in range(Y):
            hosend[k, :, h * 128 : (h + 1) * 128] = res[k * rows : (k + 1) * rows]
    o_copies = []
    for n, d in enumerate((2, 1, 3)):
        c = copy_to(hosend.at[yy(d)], ho.at[y], o_send.at[n], o_recv.at[n], tp=yy(d))
        c.start()
        o_copies.append(c)
    ho[y] = hosend[y]
    for c in wo_sends[2:] + wo_forward:
        c.wait_recv()
    for c in o_copies:
        c.wait_recv()
    for b in range(Y):
        cols = pl.ds(b * cb, cb)
        acc = jnp.zeros((rows, cb), F32)
        for k in range(Y):
            acc = acc + jnp.dot(ho[k], wo[k, :, cols], preferred_element_type=F32)
        out[:, cols] = (latent[:, cols].astype(F32) + full[b, 2:3, :] * acc).astype(BF16)

    for c in stage1 + stage2 + stage3 + lat_sends + lat_forward + wo_sends + wo_forward + o_copies:
        c.wait_send()
    for s in range(last - 1):
        for direction in (1, -1):
            for which in (0, 1):
                ring(s, direction, which).wait_send()
    ring(last - 1, 1, 0).wait_send()
    ring(last - 1, -1, 1).wait_send()


def on_device(
    sizes, latent, context, cond, context_cond, norm_gain, mod_shift, mod_scale, mod_gate, w_query, w_key, w_value,
    query_gain, key_gain, mix_lambda, context_lift, value_gain, w_out,
):
    Z, Y = sizes
    rows, D = latent.shape
    cr = context.shape[0]
    LR = Y * rows
    width = w_query.shape[1]
    heads = width // 128
    cb = mod_shift.shape[1]
    rope = jnp.asarray(rope_table(query_gain.shape[0]))
    vmem = pl.BlockSpec(memory_space=pltpu.VMEM)
    smem = pl.BlockSpec(memory_space=pltpu.SMEM)
    anys = pl.BlockSpec(memory_space=pl.ANY)
    dma = pltpu.SemaphoreType.DMA
    V = pltpu.VMEM
    return pl.pallas_call(
        functools.partial(kernel, sizes),
        out_shape=jax.ShapeDtypeStruct((rows, D), BF16),
        in_specs=[vmem] * 11 + [smem] * 2 + [vmem] + [anys] * 4,
        out_specs=vmem,
        scratch_shapes=[
            V((D, width), BF16), V((D, width), BF16), V((D, width), BF16), V((Y, w_out.shape[0], D), BF16),
            V((Y, rows, D), BF16), V((LR + cr, D), BF16), V((LR + cr, 128), F32),
            V((7, 8, cb), F32), V((2, 8, cb), F32), V((3, 8, cb), F32), V((Y, 8, cb), F32),
            V((LR + cr, 128), F32), V((LR + cr, 128), F32),
            V((heads, 2 * LR, 128), BF16), V((Z, LR + cr, width), BF16), V((Z, LR + cr, width), BF16),
            V((heads, 2 * LR, 128), F32), V((heads, 2 * LR, 128), F32),
            V((Y, rows, width), BF16), V((Y, rows, width), BF16),
            dma((4,)), dma((6,)), dma((6,)), dma((3,)), dma((3,)), dma((3,)), dma((3,)), dma((6,)), dma((6,)),
            dma((6,)), dma((6,)), dma((2, 2, Z // 2)), dma((2, 2, Z // 2)), dma((3,)), dma((3,)),
        ],
        compiler_params=pltpu.CompilerParams(
            collective_id=0, has_side_effects=True, vmem_limit_bytes=48 * 1024 * 1024
        ),
    )(
        latent, context, cond.reshape(1, -1), context_cond.reshape(1, -1), norm_gain.reshape(1, -1),
        mod_shift, mod_scale, mod_gate, query_gain.reshape(1, -1), key_gain.reshape(1, -1), value_gain.reshape(1, -1),
        mix_lambda, context_lift, rope, w_query, w_key, w_value, w_out,
    )


def solution(mesh):
    placed = (
        P(("dp", "sp", "tp"), None),
        P(("dp", "sp"), None),
        P(("dp", "sp")),
        P("sp"),
        P(),
        P("sp", "tp"),
        P("sp", "tp"),
        P("sp", "tp"),
        P(None, "tp"),
        P(None, "tp"),
        P(None, "tp"),
        P(),
        P(),
        P("tp"),
        P("tp"),
        P(),
        P("tp", None),
    )
    sizes = (mesh.shape["sp"], mesh.shape["tp"])
    return jax.shard_map(
        functools.partial(on_device, sizes),
        mesh=mesh,
        in_specs=placed,
        out_specs=P(("dp", "sp", "tp"), None),
        check_vma=False,
    )
```

time: 232 us -> 97.1 us (0.42)
  waiting for transfers between devices: 114 us -> 0 us
  Pallas kernels: 0 us -> 84.2 us
  blocking collectives: 21.2 us -> 0 us
  other arithmetic: 19.8 us -> 0 us
  starting transfers between devices: 19.8 us -> 0 us
  matrix products: 17.8 us -> 0 us
  between operations: 13.8 us -> 0.06 us
  local copies, waits for them, and re-layouts: 24.7 us -> 12.4 us
    all_gather x2 -> x0, waiting for transfers between devices: 96.5 us -> none  [the longest x1 77.1 us: sent_together(): lax.all_gather(both, axis, axis=dim, tiled=True)]
    pallas_call x0 -> x1, Pallas kernels: none -> 84.2 us  [on_device(): pl.pallas_call(functools.partial(kernel, sizes), out_shape=jax.ShapeDtype...]
    all_to_all x1 -> x0, blocking collectives: 21.2 us -> none  [sum_at_owner(): lax.all_to_all(cut_along(array, dim, devices), axis, 0, 0, tiled=True)]
    all_to_all x2 -> x0, starting transfers between devices: 19.7 us -> none  [copy_for_each(): return lax.all_to_all(copies, axis, split_axis=0, concat_axis=0, tiled=True)]
    dot_general x27 -> x0, matrix products: 17.8 us -> none  [the longest x9 4.96 us: accumulate(): jnp.einsum('qhmd,phmd->mhqp', shaped_query, shaped_keys, preferred_elemen...]
    all_to_all x2 -> x0, waiting for transfers between devices: 17.3 us -> none  [copy_for_each(): return lax.all_to_all(copies, axis, split_axis=0, concat_axis=0, tiled=True)]
    unnamed x42 -> x37, local copies, waits for them, and re-layouts: 0.53 us -> 12.4 us
    dynamic_slice x24 -> x0, local copies, waits for them, and re-layouts: 10.8 us -> none  [accumulate_blocks(): running = lax.scan(scan_step, running, slabs)[0]]
  transfers between devices with their start and end apart: 4 -> 0, of which waited for: 4 -> 0; matrix products, arithmetic and copies ran while one was open for 7% -> 0% of each run, Pallas kernels for 0% -> 0%
where the time goes in v1:
time: 97.1 us; the launch traced here: 96.7 us
  Pallas kernels  84.2 us (87%)
  local copies, waits for them, and re-layouts  12.4 us (13%)
    pallas_call x1, Pallas kernels, on_device(): pl.pallas_call(functools.partial(kernel, sizes), out_shape=jax.ShapeDtype...  84.2 us
    unnamed x37, local copies, waits for them, and re-layouts  12.4 us

profile of v1, /device:TPU:6, one launch (start us, length us, event | category | flops | bytes accessed | tf_op | source)
XLA Modules:
  0.0 96.7 jit_solution(16730971769315262257)
XLA Ops:
  0.0 0.0 copy-start.10
  0.0 0.0 copy-start.14
  0.0 0.0 copy-start.15
  0.0 0.0 copy-start.16
  0.0 0.0 copy-start.11
  0.0 0.0 copy-start.12
  0.0 0.0 copy-start.13
  0.0 0.6 copy-done.10
  0.7 0.0 copy-done.14
  0.7 0.0 copy-done.15
  0.7 0.0 copy-done.16
  0.7 0.0 copy-done.11
  0.7 0.0 copy-done.12
  0.7 0.0 copy-done.13
  0.8 0.0 copy-start
  0.8 1.2 %copy-done = bf16[2048,256]{1,0:T(8,128)(2,1)S(1)} copy-done((bf16[2048,256]{1,0:T(8,128)(2,1)S(1)}, bf16[2048,256]{1,0:T(8,128)(2,1)}, u32[]{:S(2)}) %copy-start) | copy-done | bytes 1048600
  2.0 0.0 copy-start.1
  2.0 1.2 %copy-done.1 = bf16[2048,256]{1,0:T(8,128)(2,1)S(1)} copy-done((bf16[2048,256]{1,0:T(8,128)(2,1)S(1)}, bf16[2048,256]{1,0:T(8,128)(2,1)}, u32[]{:S(2)}) %copy-start.1) | copy-done | bytes 1048600
  3.2 0.0 copy-start.2
  3.2 1.2 %copy-done.2 = bf16[2048,256]{1,0:T(8,128)(2,1)S(1)} copy-done((bf16[2048,256]{1,0:T(8,128)(2,1)S(1)}, bf16[2048,256]{1,0:T(8,128)(2,1)}, u32[]{:S(2)}) %copy-start.2) | copy-done | bytes 1048600
  4.4 0.0 copy-start.3
  4.4 1.2 %copy-done.3 = bf16[256,2048]{1,0:T(8,128)(2,1)S(1)} copy-done((bf16[256,2048]{1,0:T(8,128)(2,1)S(1)}, bf16[256,2048]{1,0:T(8,128)(2,1)}, u32[]{:S(2)}) %copy-start.3) | copy-done | bytes 1048600
  5.7 0.0 copy-start.4
  5.7 0.9 copy-done.4
  6.6 0.0 copy-start.5
  6.6 0.9 copy-done.5
  7.5 0.0 copy-start.6
  7.5 0.9 copy-done.6
  8.4 0.0 copy-start.7
  8.4 0.9 copy-done.7
  9.3 0.0 copy-start.8
  9.3 0.9 copy-done.8
  10.2 0.0 copy-start.9
  10.2 0.8 copy-done.9
  11.1 0.0 copy-start.17
  11.1 0.7 copy-done.17
  11.7 84.2 %shard_map.172 = bf16[64,2048]{1,0:T(8,128)(2,1)S(1)} custom-call(bf16[64,2048]{1,0:T(8,128)(2,1)S(1)} %copy-done.4, bf16[16,2048]{1,0:T(8,128)(2,1)S(1)} %copy-done.9, bf16[1,128]{1,0:T(2,128)(2,1)S(1)} %bitcast.7, bf16[1,128]{1,0:T(2,128)(2,1)S(1)} %bitcast.8, f32[1,2048]{1,0:T(1,128)S(1)} %bitcast.6, bf16[128,512]{1,0:T(8,128)(2,1)S(1)} %copy-done.5, ...), custom_call_target="tpu_custom_call" | custom-call | tf_op jit(solution)/shard_map/pallas_call | solution.py:362
  96.0 0.7 copy.20
Async XLA Ops:
  0.0 0.7 copy-start.10
  0.0 0.7 copy-start.14
  0.0 0.7 copy-start.15
  0.0 0.7 copy-start.16
  0.0 0.7 copy-start.11
  0.0 0.7 copy-start.12
  0.0 0.7 copy-start.13
  0.8 1.2 %copy-start = (bf16[2048,256]{1,0:T(8,128)(2,1)S(1)}, bf16[2048,256]{1,0:T(8,128)(2,1)}, u32[]{:S(2)}) copy-start(bf16[2048,256]{1,0:T(8,128)(2,1)} %wq_h.1) | copy-start | bytes 3145732
  2.0 1.2 %copy-start.1 = (bf16[2048,256]{1,0:T(8,128)(2,1)S(1)}, bf16[2048,256]{1,0:T(8,128)(2,1)}, u32[]{:S(2)}) copy-start(bf16[2048,256]{1,0:T(8,128)(2,1)} %wk_h.1) | copy-start | bytes 3145732
  3.2 1.2 %copy-start.2 = (bf16[2048,256]{1,0:T(8,128)(2,1)S(1)}, bf16[2048,256]{1,0:T(8,128)(2,1)}, u32[]{:S(2)}) copy-start(bf16[2048,256]{1,0:T(8,128)(2,1)} %wv_h.1) | copy-start | bytes 3145732
  4.4 1.2 %copy-start.3 = (bf16[256,2048]{1,0:T(8,128)(2,1)S(1)}, bf16[256,2048]{1,0:T(8,128)(2,1)}, u32[]{:S(2)}) copy-start(bf16[256,2048]{1,0:T(8,128)(2,1)} %wo_h.1) | copy-start | bytes 3145732
  5.7 0.9 copy-start.4
  6.6 0.9 copy-start.5
  7.5 0.9 copy-start.6
  8.4 0.9 copy-start.7
  9.3 0.9 copy-start.8
  10.2 0.8 copy-start.9
  11.1 0.7 copy-start.17

commit v2 on v1

--- a/solution.py
+++ b/solution.py
@@ -376,7 +376,7 @@
             dma((6,)), dma((6,)), dma((2, 2, Z // 2)), dma((2, 2, Z // 2)), dma((3,)), dma((3,)),
         ],
         compiler_params=pltpu.CompilerParams(
-            collective_id=0, has_side_effects=True, vmem_limit_bytes=48 * 1024 * 1024
+            collective_id=0, has_side_effects=True, vmem_limit_bytes=67043328
         ),
     )(
         latent, context, cond.reshape(1, -1), context_cond.reshape(1, -1), norm_gain.reshape(1, -1),

time: 97.1 us -> 87.2 us (0.90)
  local copies, waits for them, and re-layouts: 12.4 us -> 1.67 us
  Pallas kernels: 84.2 us -> 85.4 us
    unnamed x37 -> x1, local copies, waits for them, and re-layouts: 12.4 us -> 1.67 us
    pallas_call x1, Pallas kernels: 84.2 us -> 85.4 us  [on_device(): pl.pallas_call(functools.partial(kernel, sizes), out_shape=jax.ShapeDtype...]
where the time goes in v2:
time: 87.2 us; the launch traced here: 87.1 us
  Pallas kernels  85.4 us (98%)
  local copies, waits for them, and re-layouts  1.67 us (2%)
    pallas_call x1, Pallas kernels, on_device(): pl.pallas_call(functools.partial(kernel, sizes), out_shape=jax.ShapeDtype...  85.4 us

profile of v2, /device:TPU:6, one launch (start us, length us, event | category | flops | bytes accessed | tf_op | source)
XLA Modules:
  0.0 87.1 jit_solution(6484824148052050642)
XLA Ops:
  0.0 85.4 %shard_map.172 = bf16[64,2048]{1,0:T(8,128)(2,1)} custom-call(bf16[64,2048]{1,0:T(8,128)(2,1)} %latent.1, bf16[16,2048]{1,0:T(8,128)(2,1)} %context.1, bf16[1,128]{1,0:T(2,128)(2,1)} %bitcast.7, bf16[1,128]{1,0:T(2,128)(2,1)} %bitcast.8, f32[1,2048]{1,0:T(1,128)} %bitcast.6, bf16[128,512]{1,0:T(8,128)(2,1)} %msh.1, bf16[128,512]{1,0:T(8,128)(2,1)} %msc.1, ...), custom_call_target="tpu_custom_call" | custom-call | tf_op jit(solution)/shard_map/pallas_call | solution.py:362
  85.4 1.7 %copy.20 = bf16[64,2048]{1,0:T(8,128)(2,1)} copy(bf16[64,2048]{1,0:T(8,128)(2,1)} %shard_map.172) | data formatting | bytes 524288

commit v3 on v1

v3 whole, which is shorter than its diff:
```python
import functools

import jax
import jax.numpy as jnp
import numpy as np
from jax import lax
from jax.experimental import pallas as pl
from jax.experimental.pallas import tpu as pltpu
from jax.sharding import PartitionSpec as P

GRID = 64
token_eps = 0.01
head_eps = 0.001
rope_base = 10000.0
head_factor = 0.8
MESH = pl.DeviceIdType.MESH
F32 = jnp.float32
BF16 = jnp.bfloat16


def rope_table(head_width):
    quarter = head_width // 4
    inverse = np.float32(rope_base) ** (-np.arange(quarter, dtype=np.float32) / np.float32(quarter))
    angles = (np.arange(GRID, dtype=np.float32)[:, None] * inverse).astype(np.float64)
    cos, sin = np.cos(angles), np.sin(angles)
    zero = np.zeros_like(cos)
    cos_row = np.concatenate([cos, cos, zero, zero], 1)
    cos_col = np.concatenate([zero, zero, cos, cos], 1)
    sin_row = np.concatenate([-sin, sin, zero, zero], 1)
    sin_col = np.concatenate([zero, zero, -sin, sin], 1)
    table = np.stack([np.stack([cos_row, cos_col]), np.stack([sin_row, sin_col])])
    return np.tile(table, (1, 1, 1, 2)).astype(np.float32)


def silu(v):
    return v / (1.0 + jnp.exp(-v))


def kernel(
    dims,
    latent_h, context_h, cond_h, cctx_h, gain_h, msh_h, msc_h, mga_h, qg_h, kg_h, vg_h, lam_h, lift_h, rope_h,
    wk_h, wv_h, wq_h, wo_h,
    out,
    latent, context, cond, cctx, gain, msh, msc, mga, qg, kg, vg, lam, lift, rope, wk, wv, wq,
    wo, lat, xi, xc, accs, oacc, part, sums, far, full, partn, sumsn, farn, fulln, cosb, sinb, qz, kbuf, vbuf, cbuf,
    numer, tot, hosend, ho,
    lsem, p_send, p_recv, f_send, f_recv, c_send, c_recv, y_send, y_recv, w_send, w_recv, r_send, r_recv, o_send, o_recv,
):
    Z, Y = dims
    z, y = lax.axis_index("sp"), lax.axis_index("tp")

    def zz(d):
        return lax.rem(z + (d + Z), Z)

    def yy(d):
        return lax.rem(y + (d + Y), Y)

    barrier = pltpu.get_barrier_semaphore()
    z_peers = [4, -4, 3, -3, 2, -2, 1, -1]
    for d in z_peers:
        pl.semaphore_signal(barrier, inc=1, device_id={"sp": zz(d)}, device_id_type=MESH)
    for d in (2, 1, 3):
        pl.semaphore_signal(barrier, inc=1, device_id={"tp": yy(d)}, device_id_type=MESH)

    pairs = [
        (cond_h, cond), (cctx_h, cctx), (msh_h, msh), (msc_h, msc), (mga_h, mga), (latent_h, latent), (rope_h, rope),
        (gain_h, gain), (context_h, context), (qg_h, qg), (kg_h, kg), (vg_h, vg), (lam_h, lam), (lift_h, lift),
        (wv_h, wv), (wk_h, wk), (wq_h, wq), (wo_h, wo.at[y]),
    ]
    loads = [pltpu.make_async_copy(src, dst, lsem.at[n]) for n, (src, dst) in enumerate(pairs)]
    for copy in loads:
        copy.start()
    for copy in loads[:5]:
        copy.wait()

    rows16 = lax.broadcasted_iota(jnp.int32, (16, 128), 0)
    a0 = silu(cond[...].astype(F32))
    a1 = silu(cctx[...].astype(F32))
    acts = jnp.where(rows16 == 0, a0, jnp.where(rows16 == 1, a1, 0.0)).astype(BF16)
    p_sh = jnp.dot(acts, msh[...], preferred_element_type=F32)
    p_sc = jnp.dot(acts, msc[...], preferred_element_type=F32)
    p_ga = jnp.dot(acts, mga[...], preferred_element_type=F32)
    T = msh.shape[1] // 128
    for j in range(T):
        js = slice(j * 128, (j + 1) * 128)
        part[0, j : j + 1, :] = p_sh[0:1, js]
        part[0, T + j : T + j + 1, :] = p_sc[0:1, js]
        partn[0, j : j + 1, :] = p_ga[0:1, js]
        partn[0, T + j : T + j + 1, :] = p_sh[1:2, js]
        partn[0, 2 * T + j : 2 * T + j + 1, :] = p_sc[1:2, js]
        partn[0, 3 * T + j : 3 * T + j + 1, :] = jnp.zeros((1, 128), F32)
    loads[5].wait()

    pl.semaphore_wait(barrier, len(z_peers) + 3)

    def copy_to(src, dst, ssem, rsem, **where):
        return pltpu.make_async_remote_copy(
            src_ref=src, dst_ref=dst, send_sem=ssem, recv_sem=rsem, device_id=where, device_id_type=MESH
        )

    offs = [-4, 3, -3, 2, -2, 1, -1]

    def first_stage(buf, g):
        return [
            copy_to(buf.at[0], buf.at[n + 1], p_send.at[g, n], p_recv.at[g, n], sp=zz(-d)) for n, d in enumerate(offs)
        ]

    stage1 = first_stage(part, 0)
    stage1n = first_stage(partn, 1)
    for c in stage1:
        c.start()

    rows = latent.shape[0]
    half = rows // 2
    top, bottom = pl.ds(0, half), pl.ds(half, half)

    def y_copies(src, slots, send, recv, first, second):
        return [
            copy_to(src.at[first], slots.at[y, first], send.at[0], recv.at[0], tp=yy(1)),
            copy_to(src.at[second], slots.at[y, second], send.at[1], recv.at[1], tp=yy(-1)),
            copy_to(src.at[second], slots.at[y, second], send.at[2], recv.at[2], tp=yy(1)),
            copy_to(src.at[first], slots.at[y, first], send.at[3], recv.at[3], tp=yy(-1)),
        ]

    def y_forward(slots, send, recv, first, second):
        return [
            copy_to(slots.at[yy(-1), first], slots.at[yy(-1), first], send.at[4], recv.at[4], tp=yy(1)),
            copy_to(slots.at[yy(1), second], slots.at[yy(1), second], send.at[5], recv.at[5], tp=yy(-1)),
        ]

    lat_sends = y_copies(latent, lat, y_send, y_recv, top, bottom)
    for c in lat_sends:
        c.start()
    for c in stage1n:
        c.start()

    def unit(x):
        xf = x.astype(F32)
        return xf * lax.rsqrt(jnp.mean(xf * xf, axis=-1, keepdims=True) + token_eps)

    width = wq.shape[1]
    hw = qg.shape[1]
    LR = Y * rows
    CR = context.shape[0]
    xi[y] = unit(latent[...])

    def window(buf):
        t = buf[0]
        for n in range(len(offs)):
            t = t + buf[n + 1]
        return t

    def second_stage(src, dst, g):
        return [
            copy_to(src, dst.at[n], f_send.at[g, n], f_recv.at[g, n], sp=zz(d)) for n, d in enumerate((4, -4))
        ]

    for c in stage1:
        c.wait_recv()
    sums[...] = window(part)
    stage2 = second_stage(sums, far, 0)
    for c in stage2:
        c.start()
    for c in stage1n:
        c.wait_recv()
    sumsn[...] = window(partn)
    stage2n = second_stage(sumsn, farn, 1)
    for c in stage2n:
        c.start()

    lat_sends[0].wait_recv()
    lat_sends[1].wait_recv()
    lat_forward = y_forward(lat, y_send, y_recv, top, bottom)
    for c in lat_forward:
        c.start()

    gi = lax.broadcasted_iota(jnp.int32, (width, width), 0) // hw
    gj = lax.broadcasted_iota(jnp.int32, (width, width), 1) // hw
    average = jnp.where(gi == gj, 1.0 / hw, 0.0).astype(BF16)
    for copy in loads[6:14]:
        copy.wait()
    for k in range(Y):
        at = pl.ds(k * rows, rows)
        cosb[at, :] = rope[0, 0, pl.ds(Y * z + k, 1), :] + rope[0, 1]
        sinb[at, :] = rope[1, 0, pl.ds(Y * z + k, 1), :] + rope[1, 1]
    xc[...] = unit(context[...])
    lat_sends[2].wait_recv()
    lat_sends[3].wait_recv()
    for d in (1, -1):
        xi[yy(d)] = unit(lat[yy(d)])

    def third_stage(buf, g):
        return [
            copy_to(buf.at[y], buf.at[y], c_send.at[g, n], c_recv.at[g, n], tp=yy(d)) for n, d in enumerate((2, 1, 3))
        ]

    for c in stage2:
        c.wait_recv()
    full[y] = far[0] + far[1]
    stage3 = third_stage(full, 0)
    for c in stage3:
        c.start()
    for c in lat_forward:
        c.wait_recv()
    xi[yy(2)] = unit(lat[yy(2)])
    for copy in loads[14:17]:
        copy.wait()

    cb = T * 128

    def row_of(buf, b, r):
        return jnp.concatenate([buf[b, r * T + j : r * T + j + 1, :] for j in range(T)], axis=1)

    def columns(b):
        return pl.ds(pl.multiple_of(b * cb, cb), cb)

    def modulated(b):
        at = columns(b)
        scaled = gain[:, at] * (1.0 + row_of(full, b, 1))
        return (xi[:, :, at].reshape(LR, cb) * scaled + row_of(full, b, 0)).astype(BF16)

    def product(part_rows, weight, b):
        return jnp.dot(part_rows, weight[columns(b), :], preferred_element_type=F32)

    block = modulated(y)
    for n, weight in enumerate((wv, wk, wq)):
        accs[n] = product(block, weight, y)
    for m, d in ((2, -3), (1, -1)):
        stage3[m].wait_recv()
        block = modulated(yy(d))
        for n, weight in enumerate((wv, wk, wq)):
            accs[n] = accs[n] + product(block, weight, yy(d))
    stage3[0].wait_recv()
    block = modulated(yy(2))

    lane = lax.broadcasted_iota(jnp.int32, (1, 128), 1)
    q4 = hw // 4
    is_x = (lane // q4) % 2 == 0

    def head_norm(u, g):
        sq = u * u
        hi = sq.astype(BF16)
        lo = (sq - hi.astype(F32)).astype(BF16)
        ms = jnp.dot(hi, average, preferred_element_type=F32) + jnp.dot(lo, average, preferred_element_type=F32)
        return u * lax.rsqrt(ms + token_eps) * g

    def turn(t):
        other = jnp.where(is_x, pltpu.roll(t, 128 - q4, 1), pltpu.roll(t, q4, 1))
        return t * cosb[...] + other * sinb[...]

    heads = width // 128
    last = Z // 2

    def ring(step, direction, which):
        buf = (kbuf, vbuf, cbuf)[which]
        side = 0 if direction == 1 else 1
        if direction == 1:
            src, dst = step, step + 1
        elif isinstance(step, int):
            src = 0 if step == 0 else last + step
            dst = last if step == last - 1 else last + step + 1
        else:
            src, dst = last + step, last + step + 1
        return copy_to(
            buf.at[src], buf.at[dst], r_send.at[side, which, step], r_recv.at[side, which, step], sp=zz(direction)
        )

    vbuf[0] = (accs[0] + product(block, wv, yy(2))).astype(BF16)
    for direction in (1, -1):
        ring(0, direction, 1).start()
    gk = jnp.concatenate([kg[...]] * (width // hw), axis=1)
    u = head_norm(accs[1] + product(block, wk, yy(2)), gk)
    for h in range(heads):
        kbuf[0, :, h * 128 : (h + 1) * 128] = turn(u[:, h * 128 : (h + 1) * 128]).astype(BF16)
    for direction in (1, -1):
        ring(0, direction, 0).start()

    for c in stage2n:
        c.wait_recv()
    fulln[y] = farn[0] + farn[1]
    stage3n = third_stage(fulln, 1)
    for c in stage3n:
        c.start()

    gq = jnp.concatenate([qg[...]] * (width // hw), axis=1)
    u = head_norm(accs[2] + product(block, wq, yy(2)), gq)
    for h in range(heads):
        t = turn(u[:, h * 128 : (h + 1) * 128]) * (hw ** -0.5)
        qz[h, pl.ds(0, LR), :] = jnp.where(lane < hw, t, 0.0).astype(BF16)
        qz[h, pl.ds(LR, LR), :] = jnp.where(lane < hw, 0.0, t).astype(BF16)

    for c in stage3n:
        c.wait_recv()
    own = jnp.concatenate(
        [
            (
                xc[:, b * cb : (b + 1) * cb] * (gain[:, b * cb : (b + 1) * cb] * (1.0 + row_of(fulln, b, 2)))
                + row_of(fulln, b, 1)
            ).astype(BF16)
            for b in range(Y)
        ],
        axis=1,
    )
    u = head_norm(jnp.dot(own, wk[...], preferred_element_type=F32), gk)
    cbuf[0, :, 0:width] = u.astype(BF16)
    cbuf[0, :, width : 2 * width] = jnp.dot(own, wv[...], preferred_element_type=F32).astype(BF16)
    for direction in (1, -1):
        ring(0, direction, 2).start()

    wh = wo.shape[1] // 2
    loads[17].wait()
    wo_sends = y_copies(wo.at[y], wo, w_send, w_recv, pl.ds(0, wh), pl.ds(wh, wh))
    for c in wo_sends:
        c.start()

    numer[...] = jnp.zeros_like(numer)
    tot[...] = jnp.zeros_like(tot)

    def attend(h, keys, values, extra):
        s = lax.dot_general(qz[h], keys, (((1,), (1,)), ((), ())), preferred_element_type=F32)
        if extra is not None:
            s = s + extra
        w = jnp.exp(s)
        t = w[:, 0:128]
        for j in range(1, w.shape[1] // 128):
            t = t + w[:, j * 128 : (j + 1) * 128]
        tot[h] = tot[h] + t
        numer[h] = numer[h] + jnp.dot(w.astype(BF16), values, preferred_element_type=F32)

    def attend_head(slot, h):
        hc = slice(h * 128, (h + 1) * 128)
        attend(h, kbuf[slot, :, hc], vbuf[slot, :, hc], None)

    def attend_context(low, high):
        for h in range(heads):
            keys = cbuf[low:high, :, h * 128 : (h + 1) * 128].reshape((high - low) * CR, 128)
            values = cbuf[low:high, :, width + h * 128 : width + (h + 1) * 128].reshape((high - low) * CR, 128)
            attend(h, keys, values, lift[:, h : h + 1])

    def receive(s, direction, which, forward=True):
        ring(s - 1, direction, which).wait_recv()
        if forward:
            ring(s, direction, which).start()

    def pass_on(s, units):
        for n, (which, direction) in enumerate(((1, 1), (1, -1), (0, 1), (0, -1))):
            receive(s, direction, which)
            if n < len(units):
                attend_head(*units[n])
        for direction in (1, -1):
            receive(s, direction, 2)

    def earlier(s):
        return [(slot, h) for slot in (s - 1, last + s - 1) for h in range(heads)]

    def hop(s, carry):
        pass_on(s, earlier(s))
        return carry

    mid = last // 2
    pass_on(1, [(0, h) for h in range(heads)])
    lax.fori_loop(2, mid, hop, 0)
    wo_sends[0].wait_recv()
    wo_sends[1].wait_recv()
    wo_forward = y_forward(wo, w_send, w_recv, pl.ds(0, wh), pl.ds(wh, wh))
    for c in wo_forward:
        c.start()
    lax.fori_loop(mid, last - 1, hop, 0)
    s = last - 1
    units = earlier(s)
    receive(s, -1, 1)
    attend_head(*units[0])
    receive(s, 1, 0)
    receive(s, 1, 2)
    attend_head(*units[1])
    receive(s, 1, 1, False)
    receive(s, -1, 0, False)
    receive(s, -1, 2, False)
    for slot, h in units[2:] + earlier(s + 1):
        attend_head(slot, h)
    attend_context(0, last)
    ring(s, -1, 1).wait_recv()
    ring(s, 1, 0).wait_recv()
    for h in range(heads):
        attend_head(last, h)
    ring(s, 1, 2).wait_recv()
    attend_context(last, Z)

    for h in range(heads):
        total = jnp.sum(tot[h], axis=-1, keepdims=True)
        ratio = numer[h] / total
        mixed = ratio[0:LR] - lam[:, h : h + 1] * ratio[LR : 2 * LR]
        ms = jnp.mean(mixed * mixed, axis=-1, keepdims=True)
        res = (mixed * lax.rsqrt(ms + head_eps) * vg[...] * head_factor).astype(BF16)
        for k in range(Y):
            hosend[k, :, h * 128 : (h + 1) * 128] = res[k * rows : (k + 1) * rows]
    o_copies = []
    for n, d in enumerate((2, 1, 3)):
        c = copy_to(hosend.at[yy(d)], ho.at[y], o_send.at[n], o_recv.at[n], tp=yy(d))
        c.start()
        o_copies.append(c)
    for c in wo_sends[2:] + wo_forward:
        c.wait_recv()
    oacc[...] = jnp.dot(hosend[y], wo[y], preferred_element_type=F32)
    for m, d in ((2, -3), (1, -1)):
        o_copies[m].wait_recv()
        oacc[...] = oacc[...] + jnp.dot(ho[yy(d)], wo[yy(d)], preferred_element_type=F32)
    o_copies[0].wait_recv()
    for b in range(Y):
        cols = pl.ds(b * cb, cb)
        acc = oacc[:, cols] + jnp.dot(ho[yy(2)], wo[yy(2), :, cols], preferred_element_type=F32)
        out[:, cols] = (latent[:, cols].astype(F32) + row_of(fulln, b, 0) * acc).astype(BF16)

    sent = stage1 + stage1n + stage2 + stage2n + stage3 + stage3n + lat_sends + lat_forward + wo_sends + wo_forward
    for c in sent + o_copies:
        c.wait_send()
    for s in range(last - 1):
        for direction in (1, -1):
            for which in (0, 1, 2):
                ring(s, direction, which).wait_send()
    ring(last - 1, 1, 0).wait_send()
    ring(last - 1, 1, 2).wait_send()
    ring(last - 1, -1, 1).wait_send()


def on_device(
    sizes, latent, context, cond, context_cond, norm_gain, mod_shift, mod_scale, mod_gate, w_query, w_key, w_value,
    query_gain, key_gain, mix_lambda, context_lift, value_gain, w_out,
):
    Z, Y = sizes
    rows, D = latent.shape
    cr = context.shape[0]
    LR = Y * rows
    width = w_query.shape[1]
    heads = width // 128
    rope = jnp.asarray(rope_table(query_gain.shape[0]))
    hbm = pl.BlockSpec(memory_space=pltpu.HBM)
    dma = pltpu.SemaphoreType.DMA
    V = pltpu.VMEM
    hb = lambda a: pltpu.with_memory_space_constraint(a, pltpu.HBM)
    operands = tuple(hb(a) for a in (
        latent, context, cond.reshape(1, -1), context_cond.reshape(1, -1), norm_gain.reshape(1, -1),
        mod_shift, mod_scale, mod_gate, query_gain.reshape(1, -1), key_gain.reshape(1, -1), value_gain.reshape(1, -1),
        mix_lambda.reshape(1, -1), context_lift.reshape(1, -1), rope, w_key, w_value, w_query, w_out,)
    )
    crit = 2 * mod_shift.shape[1] // 128
    rest = 2 * crit
    return pl.pallas_call(
        functools.partial(kernel, sizes),
        out_shape=jax.ShapeDtypeStruct((rows, D), BF16),
        in_specs=[hbm] * len(operands),
        out_specs=pl.BlockSpec(memory_space=pltpu.VMEM),
        scratch_shapes=[V(a.shape, a.dtype) for a in operands[:-1]]
        + [
            V((Y, w_out.shape[0], D), BF16),
            V((Y, rows, D), BF16), V((Y, rows, D), F32), V((cr, D), F32), V((3, LR, width), F32), V((rows, D), F32),
            V((8, crit, 128), F32), V((crit, 128), F32), V((2, crit, 128), F32), V((Y, crit, 128), F32),
            V((8, rest, 128), F32), V((rest, 128), F32), V((2, rest, 128), F32), V((Y, rest, 128), F32),
            V((LR, 128), F32), V((LR, 128), F32),
            V((heads, 2 * LR, 128), BF16), V((Z, LR, width), BF16), V((Z, LR, width), BF16), V((Z, cr, 2 * width), BF16),
            V((heads, 2 * LR, 128), F32), V((heads, 2 * LR, 128), F32),
            V((Y, rows, width), BF16), V((Y, rows, width), BF16),
            dma((len(operands),)), dma((2, 7)), dma((2, 7)), dma((2, 2)), dma((2, 2)), dma((2, 3)), dma((2, 3)),
            dma((6,)), dma((6,)), dma((6,)), dma((6,)), dma((2, 3, Z // 2)), dma((2, 3, Z // 2)), dma((3,)), dma((3,)),
        ],
        compiler_params=pltpu.CompilerParams(
            collective_id=0, has_side_effects=True, vmem_limit_bytes=48 * 1024 * 1024
        ),
    )(*operands)


def solution(mesh):
    placed = (
        P(("dp", "sp", "tp"), None),
        P(("dp", "sp"), None),
        P(("dp", "sp")),
        P("sp"),
        P(),
        P("sp", "tp"),
        P("sp", "tp"),
        P("sp", "tp"),
        P(None, "tp"),
        P(None, "tp"),
        P(None, "tp"),
        P(),
        P(),
        P("tp"),
        P("tp"),
        P(),
        P("tp", None),
    )
    sizes = (mesh.shape["sp"], mesh.shape["tp"])
    return jax.shard_map(
        functools.partial(on_device, sizes),
        mesh=mesh,
        in_specs=placed,
        out_specs=P(("dp", "sp", "tp"), None),
        check_vma=False,
    )
```

time: 97.1 us -> 80.9 us (0.83)
  local copies, waits for them, and re-layouts: 12.4 us -> 0.71 us
  Pallas kernels: 84.2 us -> 80.1 us
    unnamed x37 -> x1, local copies, waits for them, and re-layouts: 12.4 us -> 0.71 us
    pallas_call x1, Pallas kernels: 84.2 us -> 80.1 us  [on_device(): pl.pallas_call(functools.partial(kernel, sizes), out_shape=jax.ShapeDtype...]
where the time goes in v3:
time: 80.9 us; the launch traced here: 80.8 us
  Pallas kernels  80.1 us (99%)
    pallas_call x1, Pallas kernels, on_device(): pl.pallas_call(functools.partial(kernel, sizes), out_shape=jax.ShapeDtype...  80.1 us

profile of v3, /device:TPU:6, one launch (start us, length us, event | category | flops | bytes accessed | tf_op | source)
XLA Modules:
  0.0 80.8 jit_solution(9322356159305998247)
XLA Ops:
  0.0 80.1 %shard_map.172 = bf16[64,2048]{1,0:T(8,128)(2,1)S(1)} custom-call(bf16[64,2048]{1,0:T(8,128)(2,1)} %latent_h.1, bf16[16,2048]{1,0:T(8,128)(2,1)} %context_h.1, bf16[1,128]{1,0:T(2,128)(2,1)} %bitcast.9, bf16[1,128]{1,0:T(2,128)(2,1)} %bitcast.10, f32[1,2048]{1,0:T(1,128)} %bitcast.8, bf16[128,512]{1,0:T(8,128)(2,1)} %msh_h.1, bf16[128,512]{1,0:T(8,128)(2,1)} %msc_h.1, ...), custom_call_target="tpu_custom_call" | custom-call | tf_op jit(solution)/shard_map/pallas_call | solution.py:448
  80.1 0.7 copy.20

commit v4 on v3

--- a/solution.py
+++ b/solution.py
@@ -41,10 +41,11 @@
     latent_h, context_h, cond_h, cctx_h, gain_h, msh_h, msc_h, mga_h, qg_h, kg_h, vg_h, lam_h, lift_h, rope_h,
     wk_h, wv_h, wq_h, wo_h,
     out,
-    latent, context, cond, cctx, gain, msh, msc, mga, qg, kg, vg, lam, lift, rope, wk, wv, wq,
-    wo, lat, xi, xc, accs, oacc, part, sums, far, full, partn, sumsn, farn, fulln, cosb, sinb, qz, kbuf, vbuf, cbuf,
+    latent, cond, cctx, gain, msh, msc, mga, qg, kg, vg, lam, lift, rope, wk, wv, wq,
+    wo, lat, xi, accs, oacc, part, sums, far, full, partn, sumsn, farn, fulln, cosb, sinb, qz, kbuf, vbuf, ctxg, cinv, caccs, kctx, vctx,
     numer, tot, hosend, ho,
     lsem, p_send, p_recv, f_send, f_recv, c_send, c_recv, y_send, y_recv, w_send, w_recv, r_send, r_recv, o_send, o_recv,
+    x_send, x_recv, g_send, g_recv,
 ):
     Z, Y = dims
     z, y = lax.axis_index("sp"), lax.axis_index("tp")
@@ -54,6 +55,12 @@
 
     def yy(d):
         return lax.rem(y + (d + Y), Y)
+
+    T = msh.shape[1] // 128
+    cb = T * 128
+
+    def columns(b):
+        return pl.ds(pl.multiple_of(b * cb, cb), cb)
 
     barrier = pltpu.get_barrier_semaphore()
     z_peers = [4, -4, 3, -3, 2, -2, 1, -1]
@@ -63,8 +70,8 @@
         pl.semaphore_signal(barrier, inc=1, device_id={"tp": yy(d)}, device_id_type=MESH)
 
     pairs = [
-        (cond_h, cond), (cctx_h, cctx), (msh_h, msh), (msc_h, msc), (mga_h, mga), (latent_h, latent), (rope_h, rope),
-        (gain_h, gain), (context_h, context), (qg_h, qg), (kg_h, kg), (vg_h, vg), (lam_h, lam), (lift_h, lift),
+        (cond_h, cond), (cctx_h, cctx), (msh_h, msh), (msc_h, msc), (mga_h, mga), (latent_h, latent),
+        (context_h.at[:, columns(y)], ctxg.at[y, 0]), (rope_h, rope), (gain_h, gain), (qg_h, qg), (kg_h, kg), (vg_h, vg), (lam_h, lam), (lift_h, lift),
         (wv_h, wv), (wk_h, wk), (wq_h, wq), (wo_h, wo.at[y]),
     ]
     loads = [pltpu.make_async_copy(src, dst, lsem.at[n]) for n, (src, dst) in enumerate(pairs)]
@@ -80,7 +87,6 @@
     p_sh = jnp.dot(acts, msh[...], preferred_element_type=F32)
     p_sc = jnp.dot(acts, msc[...], preferred_element_type=F32)
     p_ga = jnp.dot(acts, mga[...], preferred_element_type=F32)
-    T = msh.shape[1] // 128
     for j in range(T):
         js = slice(j * 128, (j + 1) * 128)
         part[0, j : j + 1, :] = p_sh[0:1, js]
@@ -141,7 +147,7 @@
     width = wq.shape[1]
     hw = qg.shape[1]
     LR = Y * rows
-    CR = context.shape[0]
+    CR = ctxg.shape[2]
     xi[y] = unit(latent[...])
 
     def window(buf):
@@ -168,6 +174,18 @@
     for c in stage2n:
         c.start()
 
+    reach = 4
+    loads[6].wait()
+
+    def context_copy(src, dst, to):
+        return copy_to(ctxg.at[y, src], ctxg.at[y, dst], x_send.at[dst], x_recv.at[dst], sp=zz(to))
+
+    near = {}
+    for d in range(reach, 0, -1):
+        for o in (d, Z - d):
+            near[o] = context_copy(0, o, -o if o <= reach else Z - o)
+            near[o].start()
+
     lat_sends[0].wait_recv()
     lat_sends[1].wait_recv()
     lat_forward = y_forward(lat, y_send, y_recv, top, bottom)
@@ -177,13 +195,12 @@
     gi = lax.broadcasted_iota(jnp.int32, (width, width), 0) // hw
     gj = lax.broadcasted_iota(jnp.int32, (width, width), 1) // hw
     average = jnp.where(gi == gj, 1.0 / hw, 0.0).astype(BF16)
-    for copy in loads[6:14]:
+    for copy in loads[7:14]:
         copy.wait()
     for k in range(Y):
         at = pl.ds(k * rows, rows)
         cosb[at, :] = rope[0, 0, pl.ds(Y * z + k, 1), :] + rope[0, 1]
         sinb[at, :] = rope[1, 0, pl.ds(Y * z + k, 1), :] + rope[1, 1]
-    xc[...] = unit(context[...])
     lat_sends[2].wait_recv()
     lat_sends[3].wait_recv()
     for d in (1, -1):
@@ -200,19 +217,20 @@
     stage3 = third_stage(full, 0)
     for c in stage3:
         c.start()
+    near[reach].wait_recv()
+    near[Z - reach].wait_recv()
+    relayed = [context_copy(reach, reach + d, -d) for d in range(1, reach + 1)]
+    relayed += [context_copy(Z - reach, Z - reach - d, d) for d in range(1, reach)]
+    for c in relayed:
+        c.start()
     for c in lat_forward:
         c.wait_recv()
     xi[yy(2)] = unit(lat[yy(2)])
     for copy in loads[14:17]:
         copy.wait()
 
-    cb = T * 128
-
     def row_of(buf, b, r):
         return jnp.concatenate([buf[b, r * T + j : r * T + j + 1, :] for j in range(T)], axis=1)
-
-    def columns(b):
-        return pl.ds(pl.multiple_of(b * cb, cb), cb)
 
     def modulated(b):
         at = columns(b)
@@ -252,7 +270,7 @@
     last = Z // 2
 
     def ring(step, direction, which):
-        buf = (kbuf, vbuf, cbuf)[which]
+        buf, h = (vbuf, kbuf)[which % 2], which // 2
         side = 0 if direction == 1 else 1
         if direction == 1:
             src, dst = step, step + 1
@@ -262,18 +280,23 @@
         else:
             src, dst = last + step, last + step + 1
         return copy_to(
-            buf.at[src], buf.at[dst], r_send.at[side, which, step], r_recv.at[side, which, step], sp=zz(direction)
+            buf.at[src, h], buf.at[dst, h], r_send.at[side, which, step], r_recv.at[side, which, step], sp=zz(direction)
         )
 
-    vbuf[0] = (accs[0] + product(block, wv, yy(2))).astype(BF16)
+    gk = jnp.concatenate([kg[...]] * (width // hw), axis=1)
+    v = accs[0] + product(block, wv, yy(2))
+    for h in range(heads):
+        vbuf[0, h] = v[:, h * 128 : (h + 1) * 128].astype(BF16)
     for direction in (1, -1):
-        ring(0, direction, 1).start()
-    gk = jnp.concatenate([kg[...]] * (width // hw), axis=1)
+        ring(0, direction, 0).start()
     u = head_norm(accs[1] + product(block, wk, yy(2)), gk)
     for h in range(heads):
-        kbuf[0, :, h * 128 : (h + 1) * 128] = turn(u[:, h * 128 : (h + 1) * 128]).astype(BF16)
-    for direction in (1, -1):
-        ring(0, direction, 0).start()
+        kbuf[0, h] = turn(u[:, h * 128 : (h + 1) * 128]).astype(BF16)
+        for direction in (1, -1):
+            if h > 0:
+                ring(0, direction, 2 * h).start()
+        for direction in (1, -1):
+            ring(0, direction, 2 * h + 1).start()
 
     for c in stage2n:
         c.wait_recv()
@@ -289,23 +312,17 @@
         qz[h, pl.ds(0, LR), :] = jnp.where(lane < hw, t, 0.0).astype(BF16)
         qz[h, pl.ds(LR, LR), :] = jnp.where(lane < hw, 0.0, t).astype(BF16)
 
+    for n, c in near.items():
+        if n not in (reach, Z - reach):
+            c.wait_recv()
+    for c in relayed:
+        c.wait_recv()
+    zh = Z // 2
+    ctx_sends = y_copies(ctxg.at[y], ctxg, g_send, g_recv, pl.ds(0, zh), pl.ds(zh, zh))
+    for c in ctx_sends:
+        c.start()
     for c in stage3n:
         c.wait_recv()
-    own = jnp.concatenate(
-        [
-            (
-                xc[:, b * cb : (b + 1) * cb] * (gain[:, b * cb : (b + 1) * cb] * (1.0 + row_of(fulln, b, 2)))
-                + row_of(fulln, b, 1)
-            ).astype(BF16)
-            for b in range(Y)
-        ],
-        axis=1,
-    )
-    u = head_norm(jnp.dot(own, wk[...], preferred_element_type=F32), gk)
-    cbuf[0, :, 0:width] = u.astype(BF16)
-    cbuf[0, :, width : 2 * width] = jnp.dot(own, wv[...], preferred_element_type=F32).astype(BF16)
-    for direction in (1, -1):
-        ring(0, direction, 2).start()
 
     wh = wo.shape[1] // 2
     loads[17].wait()
@@ -328,14 +345,7 @@
         numer[h] = numer[h] + jnp.dot(w.astype(BF16), values, preferred_element_type=F32)
 
     def attend_head(slot, h):
-        hc = slice(h * 128, (h + 1) * 128)
-        attend(h, kbuf[slot, :, hc], vbuf[slot, :, hc], None)
-
-    def attend_context(low, high):
-        for h in range(heads):
-            keys = cbuf[low:high, :, h * 128 : (h + 1) * 128].reshape((high - low) * CR, 128)
-            values = cbuf[low:high, :, width + h * 128 : width + (h + 1) * 128].reshape((high - low) * CR, 128)
-            attend(h, keys, values, lift[:, h : h + 1])
+        attend(h, kbuf[slot, h], vbuf[slot, h], None)
 
     def receive(s, direction, which, forward=True):
         ring(s - 1, direction, which).wait_recv()
@@ -343,84 +353,121 @@
             ring(s, direction, which).start()
 
     def pass_on(s, units):
-        for n, (which, direction) in enumerate(((1, 1), (1, -1), (0, 1), (0, -1))):
-            receive(s, direction, which)
-            if n < len(units):
-                attend_head(*units[n])
-        for direction in (1, -1):
-            receive(s, direction, 2)
+        per = -(-len(units) // (2 * heads))
+        for which in range(2 * heads):
+            for direction in (1, -1):
+                receive(s, direction, which)
+            for unit_of in units[which * per : (which + 1) * per]:
+                unit_of()
 
     def earlier(s):
-        return [(slot, h) for slot in (s - 1, last + s - 1) for h in range(heads)]
+        return [functools.partial(attend_head, slot, h) for h in range(heads) for slot in (s - 1, last + s - 1)]
 
     def hop(s, carry):
         pass_on(s, earlier(s))
         return carry
 
+    NC = Z * CR
+
+    def context_scale():
+        ms = jnp.zeros((NC, 1), F32)
+        for b in range(Y):
+            xf = ctxg[b].reshape(NC, cb).astype(F32)
+            ms = ms + jnp.sum(xf * xf, axis=-1, keepdims=True)
+        cinv[...] = jnp.broadcast_to(lax.rsqrt(ms / (Y * cb) + token_eps), (NC, 128))
+
+    def context_block(b):
+        at = slice(b * cb, (b + 1) * cb)
+        wide = jnp.concatenate([cinv[...]] * T, axis=1)
+        scaled = gain[:, at] * (1.0 + row_of(fulln, b, 2))
+        rows_b = (ctxg[b].reshape(NC, cb).astype(F32) * wide * scaled + row_of(fulln, b, 1)).astype(BF16)
+        for n, weight in enumerate((wv, wk)):
+            p = jnp.dot(rows_b, weight[at, :], preferred_element_type=F32)
+            caccs[n] = p if b == 0 else caccs[n] + p
+
+    def context_done():
+        kctx[...] = head_norm(caccs[1], gk).astype(BF16)
+        vctx[...] = caccs[0].astype(BF16)
+
+    def attend_context(h):
+        hs = slice(h * 128, (h + 1) * 128)
+        attend(h, kctx[:, hs], vctx[:, hs], lift[:, h : h + 1])
+
+    pass_on(1, [functools.partial(attend_head, 0, h) for h in range(heads)])
+    ctx_sends[0].wait_recv()
+    ctx_sends[1].wait_recv()
+    ctx_forward = y_forward(ctxg, g_send, g_recv, pl.ds(0, zh), pl.ds(zh, zh))
+    for c in ctx_forward:
+        c.start()
     mid = last // 2
-    pass_on(1, [(0, h) for h in range(heads)])
     lax.fori_loop(2, mid, hop, 0)
+    for c in ctx_sends[2:] + ctx_forward:
+        c.wait_recv()
+    extra = [context_scale] + [functools.partial(context_block, b) for b in range(Y)] + [context_done]
+    extra += [functools.partial(attend_context, h) for h in range(heads)]
+    pass_on(mid, [f for pair in zip(earlier(mid), extra[:4]) for f in pair])
     wo_sends[0].wait_recv()
     wo_sends[1].wait_recv()
     wo_forward = y_forward(wo, w_send, w_recv, pl.ds(0, wh), pl.ds(wh, wh))
     for c in wo_forward:
         c.start()
-    lax.fori_loop(mid, last - 1, hop, 0)
+    pass_on(mid + 1, [f for pair in zip(earlier(mid + 1), extra[4:]) for f in pair])
+    lax.fori_loop(mid + 2, last - 1, hop, 0)
     s = last - 1
     units = earlier(s)
-    receive(s, -1, 1)
-    attend_head(*units[0])
-    receive(s, 1, 0)
-    receive(s, 1, 2)
-    attend_head(*units[1])
-    receive(s, 1, 1, False)
-    receive(s, -1, 0, False)
-    receive(s, -1, 2, False)
-    for slot, h in units[2:] + earlier(s + 1):
-        attend_head(slot, h)
-    attend_context(0, last)
-    ring(s, -1, 1).wait_recv()
-    ring(s, 1, 0).wait_recv()
+    for n in range(2 * heads):
+        receive(s, 1 if n % 2 else -1, n)
+        units[n]()
+    for n in range(2 * heads):
+        receive(s, -1 if n % 2 else 1, n, False)
+    for f in earlier(s + 1):
+        f()
+
+    o_copies = []
     for h in range(heads):
+        ring(s, -1, 2 * h).wait_recv()
+        ring(s, 1, 2 * h + 1).wait_recv()
         attend_head(last, h)
-    ring(s, 1, 2).wait_recv()
-    attend_context(last, Z)
-
-    for h in range(heads):
         total = jnp.sum(tot[h], axis=-1, keepdims=True)
         ratio = numer[h] / total
         mixed = ratio[0:LR] - lam[:, h : h + 1] * ratio[LR : 2 * LR]
         ms = jnp.mean(mixed * mixed, axis=-1, keepdims=True)
         res = (mixed * lax.rsqrt(ms + head_eps) * vg[...] * head_factor).astype(BF16)
         for k in range(Y):
-            hosend[k, :, h * 128 : (h + 1) * 128] = res[k * rows : (k + 1) * rows]
-    o_copies = []
-    for n, d in enumerate((2, 1, 3)):
-        c = copy_to(hosend.at[yy(d)], ho.at[y], o_send.at[n], o_recv.at[n], tp=yy(d))
-        c.start()
-        o_copies.append(c)
+            hosend[h, k] = res[k * rows : (k + 1) * rows]
+        for n, d in enumerate((2, 1, 3)):
+            c = copy_to(hosend.at[h, yy(d)], ho.at[h, y], o_send.at[h, n], o_recv.at[h, n], tp=yy(d))
+            c.start()
+            o_copies.append(c)
     for c in wo_sends[2:] + wo_forward:
         c.wait_recv()
-    oacc[...] = jnp.dot(hosend[y], wo[y], preferred_element_type=F32)
+
+    def piece(buf, k):
+        return jnp.concatenate([buf[h, k] for h in range(heads)], axis=1)
+
+    oacc[...] = jnp.dot(piece(hosend, y), wo[y], preferred_element_type=F32)
     for m, d in ((2, -3), (1, -1)):
-        o_copies[m].wait_recv()
-        oacc[...] = oacc[...] + jnp.dot(ho[yy(d)], wo[yy(d)], preferred_element_type=F32)
-    o_copies[0].wait_recv()
+        for h in range(heads):
+            o_copies[3 * h + m].wait_recv()
+        oacc[...] = oacc[...] + jnp.dot(piece(ho, yy(d)), wo[yy(d)], preferred_element_type=F32)
+    for h in range(heads):
+        o_copies[3 * h].wait_recv()
+    lasts = piece(ho, yy(2))
     for b in range(Y):
         cols = pl.ds(b * cb, cb)
-        acc = oacc[:, cols] + jnp.dot(ho[yy(2)], wo[yy(2), :, cols], preferred_element_type=F32)
+        acc = oacc[:, cols] + jnp.dot(lasts, wo[yy(2), :, cols], preferred_element_type=F32)
         out[:, cols] = (latent[:, cols].astype(F32) + row_of(fulln, b, 0) * acc).astype(BF16)
 
     sent = stage1 + stage1n + stage2 + stage2n + stage3 + stage3n + lat_sends + lat_forward + wo_sends + wo_forward
-    for c in sent + o_copies:
+    for c in sent + o_copies + list(near.values()) + relayed + ctx_sends + ctx_forward:
         c.wait_send()
-    for s in range(last - 1):
+    for step in range(last - 1):
         for direction in (1, -1):
-            for which in (0, 1, 2):
-                ring(s, direction, which).wait_send()
-    ring(last - 1, 1, 0).wait_send()
-    ring(last - 1, 1, 2).wait_send()
-    ring(last - 1, -1, 1).wait_send()
+            for which in range(2 * heads):
+                ring(step, direction, which).wait_send()
+    for h in range(heads):
+        ring(last - 1, -1, 2 * h).wait_send()
+        ring(last - 1, 1, 2 * h + 1).wait_send()
 
 
 def on_device(
@@ -450,18 +497,21 @@
         out_shape=jax.ShapeDtypeStruct((rows, D), BF16),
         in_specs=[hbm] * len(operands),
         out_specs=pl.BlockSpec(memory_space=pltpu.VMEM),
-        scratch_shapes=[V(a.shape, a.dtype) for a in operands[:-1]]
+        scratch_shapes=[V(a.shape, a.dtype) for n, a in enumerate(operands[:-1]) if n != 1]
         + [
             V((Y, w_out.shape[0], D), BF16),
-            V((Y, rows, D), BF16), V((Y, rows, D), F32), V((cr, D), F32), V((3, LR, width), F32), V((rows, D), F32),
+            V((Y, rows, D), BF16), V((Y, rows, D), F32), V((3, LR, width), F32), V((rows, D), F32),
             V((8, crit, 128), F32), V((crit, 128), F32), V((2, crit, 128), F32), V((Y, crit, 128), F32),
             V((8, rest, 128), F32), V((rest, 128), F32), V((2, rest, 128), F32), V((Y, rest, 128), F32),
             V((LR, 128), F32), V((LR, 128), F32),
-            V((heads, 2 * LR, 128), BF16), V((Z, LR, width), BF16), V((Z, LR, width), BF16), V((Z, cr, 2 * width), BF16),
+            V((heads, 2 * LR, 128), BF16), V((Z, heads, LR, 128), BF16), V((Z, heads, LR, 128), BF16),
+            V((Y, Z, cr, D // Y), BF16), V((Z * cr, 128), F32), V((2, Z * cr, width), F32), V((Z * cr, width), BF16),
+            V((Z * cr, width), BF16),
             V((heads, 2 * LR, 128), F32), V((heads, 2 * LR, 128), F32),
-            V((Y, rows, width), BF16), V((Y, rows, width), BF16),
+            V((heads, Y, rows, 128), BF16), V((heads, Y, rows, 128), BF16),
             dma((len(operands),)), dma((2, 7)), dma((2, 7)), dma((2, 2)), dma((2, 2)), dma((2, 3)), dma((2, 3)),
-            dma((6,)), dma((6,)), dma((6,)), dma((6,)), dma((2, 3, Z // 2)), dma((2, 3, Z // 2)), dma((3,)), dma((3,)),
+            dma((6,)), dma((6,)), dma((6,)), dma((6,)), dma((2, 2 * heads, Z // 2)), dma((2, 2 * heads, Z // 2)), dma((heads, 3)), dma((heads, 3)),
+            dma((Z,)), dma((Z,)), dma((6,)), dma((6,)),
         ],
         compiler_params=pltpu.CompilerParams(
             collective_id=0, has_side_effects=True, vmem_limit_bytes=48 * 1024 * 1024

time: 80.9 us -> 88.7 us (1.096)
  Pallas kernels: 80.1 us -> 87.9 us
    pallas_call x1, Pallas kernels: 80.1 us -> 87.9 us  [on_device(): pl.pallas_call(functools.partial(kernel, sizes), out_shape=jax.ShapeDtype...]
where the time goes in v4:
time: 88.7 us; the launch traced here: 88.6 us
  Pallas kernels  87.9 us (99%)
    pallas_call x1, Pallas kernels, on_device(): pl.pallas_call(functools.partial(kernel, sizes), out_shape=jax.ShapeDtype...  87.9 us

profile of v4, /device:TPU:6, one launch (start us, length us, event | category | flops | bytes accessed | tf_op | source)
XLA Modules:
  0.0 88.6 jit_solution(8522364319717324272)
XLA Ops:
  0.0 87.9 %shard_map.172 = bf16[64,2048]{1,0:T(8,128)(2,1)S(1)} custom-call(bf16[64,2048]{1,0:T(8,128)(2,1)} %latent_h.1, bf16[16,2048]{1,0:T(8,128)(2,1)} %context_h.1, bf16[1,128]{1,0:T(2,128)(2,1)} %bitcast.9, bf16[1,128]{1,0:T(2,128)(2,1)} %bitcast.10, f32[1,2048]{1,0:T(1,128)} %bitcast.8, bf16[128,512]{1,0:T(8,128)(2,1)} %msh_h.1, bf16[128,512]{1,0:T(8,128)(2,1)} %msc_h.1, ...), custom_call_target="tpu_custom_call" | custom-call | tf_op jit(solution)/shard_map/pallas_call | solution.py:495
  87.9 0.7 copy.20

commit v5 on v3

--- a/solution.py
+++ b/solution.py
@@ -44,10 +44,11 @@
     latent, context, cond, cctx, gain, msh, msc, mga, qg, kg, vg, lam, lift, rope, wk, wv, wq,
     wo, lat, xi, xc, accs, oacc, part, sums, far, full, partn, sumsn, farn, fulln, cosb, sinb, qz, kbuf, vbuf, cbuf,
     numer, tot, hosend, ho,
-    lsem, p_send, p_recv, f_send, f_recv, c_send, c_recv, y_send, y_recv, w_send, w_recv, r_send, r_recv, o_send, o_recv,
+    lsem, p_send, p_recv, f_send, f_recv, c_send, c_recv, y_send, y_recv, w_send, w_recv, r_send, r_recv, o_send, o_recv, pace,
 ):
     Z, Y = dims
-    z, y = lax.axis_index("sp"), lax.axis_index("tp")
+    z, y, dp = lax.axis_index("sp"), lax.axis_index("tp"), lax.axis_index("dp")
+    partner = dp + 1 - 2 * lax.rem(dp, 2)
 
     def zz(d):
         return lax.rem(z + (d + Z), Z)
@@ -61,6 +62,8 @@
         pl.semaphore_signal(barrier, inc=1, device_id={"sp": zz(d)}, device_id_type=MESH)
     for d in (2, 1, 3):
         pl.semaphore_signal(barrier, inc=1, device_id={"tp": yy(d)}, device_id_type=MESH)
+
+    pl.semaphore_signal(barrier, inc=1, device_id={"dp": partner}, device_id_type=MESH)
 
     pairs = [
         (cond_h, cond), (cctx_h, cctx), (msh_h, msh), (msc_h, msc), (mga_h, mga), (latent_h, latent), (rope_h, rope),
@@ -91,7 +94,7 @@
         partn[0, 3 * T + j : 3 * T + j + 1, :] = jnp.zeros((1, 128), F32)
     loads[5].wait()
 
-    pl.semaphore_wait(barrier, len(z_peers) + 3)
+    pl.semaphore_wait(barrier, len(z_peers) + 4)
 
     def copy_to(src, dst, ssem, rsem, **where):
         return pltpu.make_async_remote_copy(
@@ -225,6 +228,13 @@
     block = modulated(y)
     for n, weight in enumerate((wv, wk, wq)):
         accs[n] = product(block, weight, y)
+    for c in stage2n:
+        c.wait_recv()
+    fulln[y] = farn[0] + farn[1]
+    stage3n = third_stage(fulln, 1)
+    for c in stage3n:
+        c.start()
+
     for m, d in ((2, -3), (1, -1)):
         stage3[m].wait_recv()
         block = modulated(yy(d))
@@ -275,19 +285,15 @@
     for direction in (1, -1):
         ring(0, direction, 0).start()
 
-    for c in stage2n:
-        c.wait_recv()
-    fulln[y] = farn[0] + farn[1]
-    stage3n = third_stage(fulln, 1)
-    for c in stage3n:
-        c.start()
-
     gq = jnp.concatenate([qg[...]] * (width // hw), axis=1)
     u = head_norm(accs[2] + product(block, wq, yy(2)), gq)
     for h in range(heads):
         t = turn(u[:, h * 128 : (h + 1) * 128]) * (hw ** -0.5)
-        qz[h, pl.ds(0, LR), :] = jnp.where(lane < hw, t, 0.0).astype(BF16)
-        qz[h, pl.ds(LR, LR), :] = jnp.where(lane < hw, 0.0, t).astype(BF16)
+        first = jnp.where(lane < hw, t, 0.0).astype(BF16)
+        second = jnp.where(lane < hw, 0.0, t).astype(BF16)
+        for k in range(Y):
+            qz[h, pl.ds(2 * k * rows, rows), :] = first[k * rows : (k + 1) * rows]
+            qz[h, pl.ds((2 * k + 1) * rows, rows), :] = second[k * rows : (k + 1) * rows]
 
     for c in stage3n:
         c.wait_recv()
@@ -316,33 +322,39 @@
     numer[...] = jnp.zeros_like(numer)
     tot[...] = jnp.zeros_like(tot)
 
-    def attend(h, keys, values, extra):
-        s = lax.dot_general(qz[h], keys, (((1,), (1,)), ((), ())), preferred_element_type=F32)
+    everyone = pl.ds(0, 2 * LR)
+
+    def attend(h, keys, values, extra, at=everyone):
+        s = lax.dot_general(qz[h, at, :], keys, (((1,), (1,)), ((), ())), preferred_element_type=F32)
         if extra is not None:
             s = s + extra
         w = jnp.exp(s)
         t = w[:, 0:128]
         for j in range(1, w.shape[1] // 128):
             t = t + w[:, j * 128 : (j + 1) * 128]
-        tot[h] = tot[h] + t
-        numer[h] = numer[h] + jnp.dot(w.astype(BF16), values, preferred_element_type=F32)
-
-    def attend_head(slot, h):
+        tot[h, at, :] = tot[h, at, :] + t
+        numer[h, at, :] = numer[h, at, :] + jnp.dot(w.astype(BF16), values, preferred_element_type=F32)
+
+    def attend_head(slot, h, at=everyone):
         hc = slice(h * 128, (h + 1) * 128)
-        attend(h, kbuf[slot, :, hc], vbuf[slot, :, hc], None)
-
-    def attend_context(low, high):
-        for h in range(heads):
-            keys = cbuf[low:high, :, h * 128 : (h + 1) * 128].reshape((high - low) * CR, 128)
-            values = cbuf[low:high, :, width + h * 128 : width + (h + 1) * 128].reshape((high - low) * CR, 128)
-            attend(h, keys, values, lift[:, h : h + 1])
+        attend(h, kbuf[slot, :, hc], vbuf[slot, :, hc], None, at)
+
+    def attend_context(h, low, high, at=everyone):
+        keys = cbuf[low:high, :, h * 128 : (h + 1) * 128].reshape((high - low) * CR, 128)
+        values = cbuf[low:high, :, width + h * 128 : width + (h + 1) * 128].reshape((high - low) * CR, 128)
+        attend(h, keys, values, lift[:, h : h + 1], at)
 
     def receive(s, direction, which, forward=True):
         ring(s - 1, direction, which).wait_recv()
         if forward:
             ring(s, direction, which).start()
 
+    def in_step():
+        pl.semaphore_signal(pace, inc=1, device_id={"dp": partner}, device_id_type=MESH)
+        pl.semaphore_wait(pace, 1)
+
     def pass_on(s, units):
+        in_step()
         for n, (which, direction) in enumerate(((1, 1), (1, -1), (0, 1), (0, -1))):
             receive(s, direction, which)
             if n < len(units):
@@ -367,6 +379,7 @@
         c.start()
     lax.fori_loop(mid, last - 1, hop, 0)
     s = last - 1
+    in_step()
     units = earlier(s)
     receive(s, -1, 1)
     attend_head(*units[0])
@@ -378,27 +391,29 @@
     receive(s, -1, 2, False)
     for slot, h in units[2:] + earlier(s + 1):
         attend_head(slot, h)
-    attend_context(0, last)
+    for h in range(heads):
+        attend_context(h, 0, last)
     ring(s, -1, 1).wait_recv()
     ring(s, 1, 0).wait_recv()
-    for h in range(heads):
-        attend_head(last, h)
-    ring(s, 1, 2).wait_recv()
-    attend_context(last, Z)
-
-    for h in range(heads):
-        total = jnp.sum(tot[h], axis=-1, keepdims=True)
-        ratio = numer[h] / total
-        mixed = ratio[0:LR] - lam[:, h : h + 1] * ratio[LR : 2 * LR]
-        ms = jnp.mean(mixed * mixed, axis=-1, keepdims=True)
-        res = (mixed * lax.rsqrt(ms + head_eps) * vg[...] * head_factor).astype(BF16)
-        for k in range(Y):
-            hosend[k, :, h * 128 : (h + 1) * 128] = res[k * rows : (k + 1) * rows]
     o_copies = []
-    for n, d in enumerate((2, 1, 3)):
-        c = copy_to(hosend.at[yy(d)], ho.at[y], o_send.at[n], o_recv.at[n], tp=yy(d))
-        c.start()
-        o_copies.append(c)
+    for n, d in enumerate((2, 1, 3, 0)):
+        k = yy(d)
+        at = pl.ds(pl.multiple_of(2 * k * rows, 2 * rows), 2 * rows)
+        for h in range(heads):
+            attend_head(last, h, at)
+        if n == 0:
+            ring(s, 1, 2).wait_recv()
+        for h in range(heads):
+            attend_context(h, last, Z, at)
+            ratio = numer[h, at, :] / jnp.sum(tot[h, at, :], axis=-1, keepdims=True)
+            mixed = ratio[0:rows] - lam[:, h : h + 1] * ratio[rows : 2 * rows]
+            ms = jnp.mean(mixed * mixed, axis=-1, keepdims=True)
+            res = mixed * lax.rsqrt(ms + head_eps) * vg[...] * head_factor
+            hosend[k, :, h * 128 : (h + 1) * 128] = res.astype(BF16)
+        if d != 0:
+            c = copy_to(hosend.at[k], ho.at[y], o_send.at[n], o_recv.at[n], tp=k)
+            c.start()
+            o_copies.append(c)
     for c in wo_sends[2:] + wo_forward:
         c.wait_recv()
     oacc[...] = jnp.dot(hosend[y], wo[y], preferred_element_type=F32)
@@ -462,6 +477,7 @@
             V((Y, rows, width), BF16), V((Y, rows, width), BF16),
             dma((len(operands),)), dma((2, 7)), dma((2, 7)), dma((2, 2)), dma((2, 2)), dma((2, 3)), dma((2, 3)),
             dma((6,)), dma((6,)), dma((6,)), dma((6,)), dma((2, 3, Z // 2)), dma((2, 3, Z // 2)), dma((3,)), dma((3,)),
+            pltpu.SemaphoreType.REGULAR,
         ],
         compiler_params=pltpu.CompilerParams(
             collective_id=0, has_side_effects=True, vmem_limit_bytes=48 * 1024 * 1024

time: 80.9 us -> 80.4 us (level)
  no operation moved by 1% of the time
where the time goes in v5:
time: 80.4 us; the launch traced here: 80.3 us
  Pallas kernels  79.6 us (99%)
    pallas_call x1, Pallas kernels, on_device(): pl.pallas_call(functools.partial(kernel, sizes), out_shape=jax.ShapeDtype...  79.6 us

profile of v5, /device:TPU:6, one launch (start us, length us, event | category | flops | bytes accessed | tf_op | source)
XLA Modules:
  0.0 80.3 jit_solution(8386565574918000447)
XLA Ops:
  0.0 79.6 %shard_map.172 = bf16[64,2048]{1,0:T(8,128)(2,1)S(1)} custom-call(bf16[64,2048]{1,0:T(8,128)(2,1)} %latent_h.1, bf16[16,2048]{1,0:T(8,128)(2,1)} %context_h.1, bf16[1,128]{1,0:T(2,128)(2,1)} %bitcast.9, bf16[1,128]{1,0:T(2,128)(2,1)} %bitcast.10, f32[1,2048]{1,0:T(1,128)} %bitcast.8, bf16[128,512]{1,0:T(8,128)(2,1)} %msh_h.1, bf16[128,512]{1,0:T(8,128)(2,1)} %msc_h.1, ...), custom_call_target="tpu_custom_call" | custom-call | tf_op jit(solution)/shard_map/pallas_call | solution.py:463
  79.6 0.7 copy.20

commit v6 on v5

--- a/solution.py
+++ b/solution.py
@@ -292,8 +292,9 @@
         first = jnp.where(lane < hw, t, 0.0).astype(BF16)
         second = jnp.where(lane < hw, 0.0, t).astype(BF16)
         for k in range(Y):
-            qz[h, pl.ds(2 * k * rows, rows), :] = first[k * rows : (k + 1) * rows]
-            qz[h, pl.ds((2 * k + 1) * rows, rows), :] = second[k * rows : (k + 1) * rows]
+            place = pl.multiple_of(lax.rem(k - y + (Y // 2 + Y), Y) * (2 * rows), 2 * rows)
+            qz[h, pl.ds(place, rows), :] = first[k * rows : (k + 1) * rows]
+            qz[h, pl.ds(place + rows, rows), :] = second[k * rows : (k + 1) * rows]
 
     for c in stage3n:
         c.wait_recv()
@@ -396,22 +397,25 @@
     ring(s, -1, 1).wait_recv()
     ring(s, 1, 0).wait_recv()
     o_copies = []
-    for n, d in enumerate((2, 1, 3, 0)):
-        k = yy(d)
-        at = pl.ds(pl.multiple_of(2 * k * rows, 2 * rows), 2 * rows)
+    for low, high in ((0, 1), (1, Y)):
+        at = pl.ds(2 * low * rows, 2 * (high - low) * rows)
         for h in range(heads):
             attend_head(last, h, at)
-        if n == 0:
+        if low == 0:
             ring(s, 1, 2).wait_recv()
         for h in range(heads):
             attend_context(h, last, Z, at)
-            ratio = numer[h, at, :] / jnp.sum(tot[h, at, :], axis=-1, keepdims=True)
-            mixed = ratio[0:rows] - lam[:, h : h + 1] * ratio[rows : 2 * rows]
-            ms = jnp.mean(mixed * mixed, axis=-1, keepdims=True)
-            res = mixed * lax.rsqrt(ms + head_eps) * vg[...] * head_factor
-            hosend[k, :, h * 128 : (h + 1) * 128] = res.astype(BF16)
-        if d != 0:
-            c = copy_to(hosend.at[k], ho.at[y], o_send.at[n], o_recv.at[n], tp=k)
+        for h in range(heads):
+            for j in range(low, high):
+                one, two = pl.ds(2 * j * rows, rows), pl.ds((2 * j + 1) * rows, rows)
+                mixed = numer[h, one, :] / jnp.sum(tot[h, one, :], axis=-1, keepdims=True) - lam[:, h : h + 1] * (
+                    numer[h, two, :] / jnp.sum(tot[h, two, :], axis=-1, keepdims=True)
+                )
+                ms = jnp.mean(mixed * mixed, axis=-1, keepdims=True)
+                res = mixed * lax.rsqrt(ms + head_eps) * vg[...] * head_factor
+                hosend[yy(j - Y // 2), :, h * 128 : (h + 1) * 128] = res.astype(BF16)
+        for n, d in ((0, 2),) if low == 0 else ((1, 1), (2, 3)):
+            c = copy_to(hosend.at[yy(d)], ho.at[y], o_send.at[n], o_recv.at[n], tp=yy(d))
             c.start()
             o_copies.append(c)
     for c in wo_sends[2:] + wo_forward:

time: 80.4 us -> 80.5 us (level)
  no operation moved by 1% of the time
where the time goes in v6:
time: 80.5 us; the launch traced here: 80.4 us
  Pallas kernels  79.7 us (99%)
    pallas_call x1, Pallas kernels, on_device(): pl.pallas_call(functools.partial(kernel, sizes), out_shape=jax.ShapeDtype...  79.7 us

profile of v6, /device:TPU:6, one launch (start us, length us, event | category | flops | bytes accessed | tf_op | source)
XLA Modules:
  0.0 80.4 jit_solution(8260722735144330103)
XLA Ops:
  0.0 79.7 %shard_map.172 = bf16[64,2048]{1,0:T(8,128)(2,1)S(1)} custom-call(bf16[64,2048]{1,0:T(8,128)(2,1)} %latent_h.1, bf16[16,2048]{1,0:T(8,128)(2,1)} %context_h.1, bf16[1,128]{1,0:T(2,128)(2,1)} %bitcast.9, bf16[1,128]{1,0:T(2,128)(2,1)} %bitcast.10, f32[1,2048]{1,0:T(1,128)} %bitcast.8, bf16[128,512]{1,0:T(8,128)(2,1)} %msh_h.1, bf16[128,512]{1,0:T(8,128)(2,1)} %msc_h.1, ...), custom_call_target="tpu_custom_call" | custom-call | tf_op jit(solution)/shard_map/pallas_call | solution.py:467
  79.7 0.7 copy.20
